TPU v7x, 32 devices: a whole 2x2x4 slice. The times are simulated.
32 devices in a mesh: sp: 8 (over z, y), tp: 4 (over x, core).
Axes of the slice: x: 2, y: 2, z: 4, core: 2. Of those that a mesh axis runs over, the one named last changes fastest.
Arguments:
- tokens: bfloat16 [2048, 2048], P('sp'), may hold values from -6 to 6
- input_norm_gain: float32 [2048], replicated, may hold values from 0.1 to 1.9
- convolution_value_weight: bfloat16 [2048, 512], P(None, 'tp'), may hold values from -0.125 to 0.125
- convolution_gate_weight: bfloat16 [2048, 512], P(None, 'tp'), may hold values from -0.125 to 0.125
- depthwise_taps_weight: float32 [31, 512], P(None, 'tp'), may hold values from -1 to 1
- convolution_group_gain: float32 [512], P('tp'), may hold values from 0.1 to 1.9
- convolution_group_shift: float32 [512], P('tp'), may hold values from -3 to 3
- receptance_weight: bfloat16 [2048, 1024], P(None, 'tp'), may hold values from -0.125 to 0.125
- key_weight: bfloat16 [2048, 1024], P(None, 'tp'), may hold values from -0.125 to 0.125
- value_weight: bfloat16 [2048, 1024], P(None, 'tp'), may hold values from -0.125 to 0.125
- decay_weight: bfloat16 [2048, 1024], P(None, 'tp'), may hold values from -0.0625 to 0.0625
- correction_rate_weight: bfloat16 [2048, 1024], P(None, 'tp'), may hold values from -0.125 to 0.125
- output_gate_weight: bfloat16 [2048, 1024], P(None, 'tp'), may hold values from -0.125 to 0.125
- key_prenorm_gain: float32 [1024], P('tp'), may hold values from 0.04 to 8
- decay_offset_bias: float32 [1024], P('tp'), may hold values from -30 to 0
- position_decay_shift: float32 [2048, 1024], P('sp', 'tp'), may hold values from -1 to 1
- extra_log_decay: float32 [2048, 1024], P('sp', 'tp'), may hold values from -0.7 to 0
- head_norm_gain: float32 [1024], P('tp'), may hold values from 0.1 to 1.9
- convolution_output_weight: bfloat16 [512, 2048], replicated, may hold values from -0.15625 to 0.15625
- attention_output_weight: bfloat16 [1024, 2048], replicated, may hold values from -0.15625 to 0.15625
Outputs:
- mixed: bfloat16 [2048, 2048], P(('sp', 'tp'))
All inputs are finite; a program needn't handle non-finite values.
Results may differ from a plain program's by a relative error of at most 0.0063.
The roundings to bfloat16 on the way count: a program that leaves them out, or rounds other values in their place, can miss the bound.
Values may be sent and summed in bfloat16 or wider, within the bound.
A program may use at most 128 MiB of HBM per device.

v0:
```python
import functools

import jax
import jax.numpy as jnp
from jax import lax
from jax.experimental import pallas as pl
from jax.experimental.pallas import tpu as pltpu
from jax.sharding import PartitionSpec as P

HEAD = 64
CHUNK = 64
PAIR = 128

NORM_EPS = 1e-06
GROUP_EPS = 1e-05
HEAD_EPS = 0.00064
KEY_EPS = 1e-06
MESH = pl.DeviceIdType.MESH
WIRE = jnp.bfloat16
VMEM_LIMIT = 60 * 1024 * 1024
F32 = jnp.float32
BF16 = jnp.bfloat16

NN = (((1,), (0,)), ((), ()))
NT = (((1,), (1,)), ((), ()))
TN = (((0,), (0,)), ((), ()))


def parts(x, count):
    out = []
    for _ in range(count - 1):
        piece = x.astype(BF16)
        out.append(piece)
        x = x - piece.astype(F32)
    out.append(x.astype(BF16))
    return out


def dot(a, b, dims=NN):
    return lax.dot_general(a, b, dims, preferred_element_type=F32)


def mm3(a, b, dims=NN):
    ah, al = parts(a, 2)
    bh, bl = parts(b, 2)
    return dot(ah, bh, dims) + (dot(ah, bl, dims) + dot(al, bh, dims))


def mm_left(a, b, dims=NN, count=2):
    pieces = [dot(piece, b, dims) for piece in parts(a, count)]
    return functools.reduce(jnp.add, pieces)


def mm_right(a, b, dims=NN, count=2):
    pieces = [dot(a, piece, dims) for piece in parts(b, count)]
    return functools.reduce(jnp.add, pieces)


PASSES = dict(qk=3, kmv=2, inv=1, rem=1, res=3, fix=1, read=3, keep=3, state=3, carry=3, enter=3)
REFINE = True


def mm(a, b, site, dims=NN):
    passes = PASSES[site]
    if passes == 1:
        return dot(a.astype(BF16), b.astype(BF16), dims)
    if passes == 2:
        return mm_left(a, b.astype(BF16), dims)
    return mm3(a, b, dims)


def iota2(rows, cols):
    return (
        lax.broadcasted_iota(jnp.int32, (rows, cols), 0),
        lax.broadcasted_iota(jnp.int32, (rows, cols), 1),
    )


def head_blocks(width):
    row, col = iota2(width, width)
    return (row // HEAD) == (col // HEAD)


def block_diagonal(stacked, width):
    tiled = jnp.concatenate([stacked] * (width // HEAD), axis=0)
    return jnp.where(head_blocks(width), tiled, jnp.zeros_like(tiled))


def layer_kernel(
    n_sp, n_tp,
    gain, kgain, bias, taps, ggain, gshift, hgain,
    tok_hbm, shift_hbm, extra_hbm, wcv, wcg, wk, wr, wd, we, wv, wg, wco, wao,
    out,
    tok, shift, extra, cv_buf, cg_buf, k_buf, r_buf, d_buf, e_buf, v_buf, g_buf, co_buf, ao_buf,
    conv_in, extended, halo, own_map, partner_map, pair_map, maps, state,
    local_read, carried, conv_out, mix_out, conv_slots, mix_slots,
    weight_sem, halo_sem, pair_sem, map_send, map_recv, conv_send, conv_recv, mix_send, mix_recv,
):
    sp, tp = lax.axis_index("sp"), lax.axis_index("tp")
    order = (
        (tok_hbm, tok), (wk, k_buf), (we, e_buf), (shift_hbm, shift), (extra_hbm, extra),
        (wd, d_buf), (wv, v_buf), (wcv, cv_buf), (wcg, cg_buf),
        (wr, r_buf), (wg, g_buf), (wco, co_buf), (wao, ao_buf),
    )
    copies = []
    for index, (source, buffer) in enumerate(order):
        copy = pltpu.make_async_copy(source, buffer, weight_sem.at[index])
        copy.start()
        copies.append(copy)
    barrier = pltpu.get_barrier_semaphore()
    for step in range(1, n_sp):
        pl.semaphore_signal(
            barrier, inc=1, device_id=(lax.rem(sp + step, n_sp), tp), device_id_type=MESH
        )
    for step in range(1, n_tp):
        pl.semaphore_signal(
            barrier, inc=1, device_id=(sp, lax.rem(tp + step, n_tp)), device_id_type=MESH
        )
    rows = tok.shape[0]
    channels = conv_in.shape[1]
    width = local_read.shape[1]
    heads = width // HEAD
    pairs = rows // PAIR
    halo_rows = halo.shape[0]
    groups = n_sp // 2
    group, parity = sp // 2, lax.rem(sp, 2)
    first_member = parity == 0
    copies[0].wait()
    x = tok[...].astype(F32)
    normed = (
        x * lax.rsqrt(jnp.mean(x * x, axis=-1, keepdims=True) + NORM_EPS) * gain[...]
    ).astype(BF16)

    def project(index):
        copies[index].wait()
        return dot(normed, order[index][1][...]).astype(BF16).astype(F32)

    key_all = project(1)
    ones = jnp.where(head_blocks(width), 1.0, 0.0).astype(BF16)
    unit = key_all * kgain[...]
    unit = unit * lax.rsqrt(mm_left(unit * unit, ones) + KEY_EPS)
    erase = unit * jax.nn.sigmoid(project(2))
    copies[3].wait()
    copies[4].wait()
    logits = project(5) + bias[...] + shift[...]
    decay = jax.nn.sigmoid(logits) * (-0.6065306597126334) + extra[...]
    row, col = iota2(PAIR, PAIR)
    same = (row // CHUNK) == (col // CHUNK)
    strict = same & (row > col)
    inclusive = same & (row >= col)
    eye = jnp.where(row == col, 1.0, 0.0)
    tri = jnp.where(inclusive, 1.0, 0.0).astype(BF16)
    cum = jnp.concatenate(
        [mm_right(tri, decay[p * PAIR:(p + 1) * PAIR], count=3) for p in range(pairs)], axis=0
    )

    def chunk_row(offset):
        return jnp.concatenate(
            [
                jnp.broadcast_to(cum[c + offset:c + offset + 1], (CHUNK, width))
                for c in range(0, rows, CHUNK)
            ],
            axis=0,
        )

    mid = chunk_row(CHUNK // 2 - 1)
    final = chunk_row(CHUNK - 1)
    before = cum - decay
    up = jnp.exp(mid - cum)
    left_unit = unit * jnp.exp(before - mid)
    right_erase = erase * up
    right_key = key_all * up
    query_unit = unit * jnp.exp(before)
    keep = jnp.exp(final - cum)
    kept_erase = erase * keep
    kept_key = key_all * keep
    value = project(6)

    units = [(h, p) for h in range(heads) for p in range(pairs)]

    def piece(values, unit_index):
        h, p = unit_index
        return values[p * PAIR:(p + 1) * PAIR, h * HEAD:(h + 1) * HEAD]

    lower, key_mix, values_of, rights = [], [], [], []
    for u in units:
        right = jnp.concatenate([piece(right_erase, u), piece(right_key, u)], axis=0)
        product = mm(piece(left_unit, u), right, "qk", NT)
        lower.append(jnp.where(strict, product[:, :PAIR], 0.0))
        key_mix.append(jnp.where(strict, product[:, PAIR:], 0.0))
        values_of.append(piece(value, u))
        rights.append(right)
    right_side = [
        -jnp.concatenate([mm(k, v, "kmv"), piece(query_unit, u)], axis=1)
        for k, v, u in zip(key_mix, values_of, units)
    ]
    first = strict & ((row // 2) == (col // 2))
    inverse = [eye - jnp.where(first, low, 0.0) for low in lower]
    size = 2
    while size < CHUNK:
        level = ((row // (2 * size)) == (col // (2 * size))) & ((row // size) > (col // size))
        inner = [mm(jnp.where(level, low, 0.0), inv, "inv") for low, inv in zip(lower, inverse)]
        inverse = [inv - mm(inv, step, "inv") for inv, step in zip(inverse, inner)]
        size *= 2
    removed = [mm(inv, rhs, "rem") for inv, rhs in zip(inverse, right_side)]
    if REFINE:
        left_over = [
            rhs - rem - mm(low, rem, "res") for rhs, rem, low in zip(right_side, removed, lower)
        ]
        removed = [
            rem + mm(inv, rest, "fix") for rem, inv, rest in zip(removed, inverse, left_over)
        ]
    eye_head = iota2(HEAD, HEAD)
    eye_head = eye_head[0] == eye_head[1]
    blocks = {}
    for h in range(heads):
        for p in range(pairs):
            index = h * pairs + p
            ke, kk = piece(kept_erase, (h, p)), piece(kept_key, (h, p))
            for half in range(PAIR // CHUNK):
                span = slice(half * CHUNK, (half + 1) * CHUNK)
                start = p * PAIR + half * CHUNK
                from_removed = mm(removed[index][span], ke[span], "keep", TN)
                base = from_removed[:HEAD] + mm(values_of[index][span], kk[span], "keep", TN)
                last = jnp.exp(final[start:start + 1, h * HEAD:(h + 1) * HEAD])
                trans = from_removed[HEAD:] + jnp.where(eye_head, last, 0.0)
                blocks[h, start // CHUNK] = (base, trans)
    priors = {}
    totals = [None] * heads
    for chunk in range(rows // CHUNK):
        for h in range(heads):
            base, trans = blocks[h, chunk]
            priors[h, chunk] = totals[h]
            if totals[h] is None:
                totals[h] = jnp.concatenate([base, trans], axis=0)
            else:
                moved = mm(totals[h], trans, "state")
                totals[h] = jnp.concatenate([moved[:HEAD] + base, moved[HEAD:]], axis=0)
    own_total = jnp.concatenate(totals, axis=1).astype(WIRE)
    own_map[...] = own_total

    pl.semaphore_wait(barrier, n_sp + n_tp - 2)
    pair_copy = pltpu.make_async_remote_copy(
        src_ref=own_map, dst_ref=partner_map, send_sem=pair_sem.at[0], recv_sem=pair_sem.at[1],
        device_id=(sp + 1 - 2 * parity, tp), device_id_type=MESH,
    )
    pair_copy.start()

    conv_value = project(7)
    conv_rows = (conv_value * jax.nn.sigmoid(project(8))).astype(BF16)
    conv_in[...] = conv_rows
    halo_copy = pltpu.make_async_remote_copy(
        src_ref=conv_in.at[pl.ds(rows - halo_rows, halo_rows)], dst_ref=halo,
        send_sem=halo_sem.at[0], recv_sem=halo_sem.at[1],
        device_id=(sp + 1, tp), device_id_type=MESH,
    )
    has_next = sp + 1 < n_sp

    @pl.when(has_next)
    def _():
        halo_copy.start()

    extended[halo_rows:, :] = conv_rows.astype(F32)

    def chain(carry, block):
        trans = block_diagonal(block[HEAD:], width)
        return mm(carry, trans, "enter")

    receptance = project(9)
    left_read = receptance * jnp.exp(cum - mid)
    query_read = receptance * jnp.exp(cum)

    pair_copy.wait()
    mine, theirs = own_total.astype(F32), partner_map[...].astype(F32)
    early = jnp.where(first_member, mine, theirs)
    late = jnp.where(first_member, theirs, mine)
    joined = chain(early, late)
    pair_map[:HEAD] = (joined[:HEAD] + late[:HEAD]).astype(WIRE)
    pair_map[HEAD:] = joined[HEAD:].astype(WIRE)

    def map_copy(ahead):
        return pltpu.make_async_remote_copy(
            src_ref=pair_map, dst_ref=maps.at[ahead],
            send_sem=map_send.at[ahead], recv_sem=map_recv.at[ahead],
            device_id=(sp + 2 * ahead, tp), device_id_type=MESH,
        )

    for ahead in range(1, groups):
        @pl.when(group + ahead < groups)
        def _():
            map_copy(ahead).start()

    @pl.when(sp > 0)
    def _():
        halo_copy.wait_recv()
        extended[:halo_rows, :] = halo[...].astype(F32)

    @pl.when(sp == 0)
    def _():
        extended[:halo_rows, :] = jnp.zeros((halo_rows, channels), F32)

    tap_count = taps.shape[0]
    total = jnp.zeros((rows, channels), F32)
    for offset in range(tap_count):
        begin = halo_rows - tap_count + 1 + offset
        total = total + taps[offset:offset + 1, :] * extended[begin:begin + rows, :]
    means = jnp.where(head_blocks(channels), 1.0 / HEAD, 0.0).astype(BF16)
    centred = total - mm_left(total, means)
    scaled = centred * lax.rsqrt(mm_left(centred * centred, means) + GROUP_EPS)
    conv_out[...] = jax.nn.silu(scaled * ggain[...] + gshift[...]).astype(BF16)

    span = rows // n_tp

    def spread(source, slots, send, recv):
        started = []
        for step in range(1, n_tp):
            target = lax.rem(tp + step, n_tp)
            begin = pl.multiple_of(target * span, span)
            copy = pltpu.make_async_remote_copy(
                src_ref=source.at[pl.ds(begin, span)], dst_ref=slots.at[step],
                send_sem=send.at[step], recv_sem=recv.at[step],
                device_id=(sp, target), device_id_type=MESH,
            )
            copy.start()
            started.append(copy)
        return started

    conv_copies = spread(conv_out, conv_slots, conv_send, conv_recv)

    zeros = jnp.zeros((PAIR, HEAD), F32)
    for index, u in enumerate(units):
        h, p = u
        product = mm(piece(left_read, u), rights[index], "qk", NT)
        mix = jnp.concatenate(
            [
                jnp.where(inclusive, product[:, :PAIR], 0.0),
                jnp.where(inclusive, product[:, PAIR:], 0.0),
            ],
            axis=1,
        )
        stacked = jnp.concatenate(
            [removed[index], jnp.concatenate([values_of[index], zeros], axis=1)], axis=0
        )
        readout = mm(mix, stacked, "read") + jnp.concatenate(
            [zeros, piece(query_read, u)], axis=1
        )
        for half in range(PAIR // CHUNK):
            start = p * PAIR + half * CHUNK
            lanes = slice(h * HEAD, (h + 1) * HEAD)
            read = readout[half * CHUNK:(half + 1) * CHUNK]
            prior = priors[h, start // CHUNK]
            if prior is not None:
                read = jnp.concatenate(
                    [read[:, :HEAD], jnp.zeros((CHUNK, HEAD), F32)], axis=1
                ) + mm(read[:, HEAD:], prior, "carry", NT)
            local_read[start:start + CHUNK, lanes] = read[:, :HEAD]
            carried[start:start + CHUNK, lanes] = read[:, HEAD:]
    gate = jax.nn.sigmoid(project(10)) * hgain[...]

    own = pl.multiple_of(tp * span, span)

    def gather(result, source, slots, arriving, weight, depth):
        result = result + dot(
            source[pl.ds(own, span)], weight[pl.ds(pl.multiple_of(tp * depth, depth), depth)]
        )
        for step in range(1, n_tp):
            arriving[step - 1].wait_recv()
            begin = lax.rem(tp - step + n_tp, n_tp) * depth
            result = result + dot(
                slots[step], weight[pl.ds(pl.multiple_of(begin, depth), depth)]
            )
        return result

    copies[11].wait()
    result = gather(
        jnp.zeros(out.shape, F32), conv_out, conv_slots, conv_copies, co_buf, channels
    )

    state[...] = jnp.zeros_like(state)
    for ahead in range(groups - 1, 0, -1):
        @pl.when(group >= ahead)
        def _():
            map_copy(ahead).wait_recv()
            block = maps[ahead].astype(F32)
            state[...] = chain(state[...], block) + block[:HEAD]

    behind = chain(state[...], early) + early[:HEAD]
    entering = jnp.where(first_member, state[...], behind)
    readout = local_read[...] + mm(carried[...], block_diagonal(entering, width), "enter", NT)
    head_means = jnp.where(head_blocks(width), 1.0 / HEAD, 0.0).astype(BF16)
    centred = readout - mm_left(readout, head_means)
    scaled = centred * lax.rsqrt(mm_left(centred * centred, head_means) + HEAD_EPS)
    mix_out[...] = (scaled * gate).astype(BF16)
    mix_copies = spread(mix_out, mix_slots, mix_send, mix_recv)
    copies[12].wait()
    result = gather(result, mix_out, mix_slots, mix_copies, ao_buf, width)
    out[...] = result.astype(BF16)
    for copy in conv_copies + mix_copies:
        copy.wait_send()

    @pl.when(has_next)
    def _():
        halo_copy.wait_send()

    for ahead in range(1, groups):
        @pl.when(group + ahead < groups)
        def _():
            map_copy(ahead).wait_send()


def local(
    n_sp, n_tp,
    tokens, input_norm_gain, convolution_value_weight, convolution_gate_weight,
    depthwise_taps_weight, convolution_group_gain, convolution_group_shift,
    receptance_weight, key_weight, value_weight, decay_weight, correction_rate_weight,
    output_gate_weight, key_prenorm_gain, decay_offset_bias, position_decay_shift,
    extra_log_decay, head_norm_gain, convolution_output_weight, attention_output_weight,
):
    rows, model = tokens.shape
    channels = convolution_value_weight.shape[1]
    width = key_weight.shape[1]
    vmem = pl.BlockSpec(memory_space=pltpu.VMEM)
    anywhere = pl.BlockSpec(memory_space=pl.ANY)

    def line(values):
        return values.reshape(1, -1)

    weights = (
        convolution_value_weight, convolution_gate_weight, key_weight, receptance_weight,
        decay_weight, correction_rate_weight, value_weight, output_gate_weight,
        convolution_output_weight, attention_output_weight,
    )
    span = rows // n_tp
    halo_rows = -(-(depthwise_taps_weight.shape[0] - 1) // 16) * 16
    groups = n_sp // 2
    dma = pltpu.SemaphoreType.DMA
    map_shape = (2 * HEAD, width)
    return pl.pallas_call(
        functools.partial(layer_kernel, n_sp, n_tp),
        name="layer",
        out_shape=jax.ShapeDtypeStruct((span, model), BF16),
        in_specs=[vmem] * 7 + [anywhere] * 13,
        out_specs=vmem,
        scratch_shapes=[
            pltpu.VMEM(tokens.shape, BF16),
            pltpu.VMEM(position_decay_shift.shape, F32),
            pltpu.VMEM(extra_log_decay.shape, F32),
        ]
        + [pltpu.VMEM(weight.shape, BF16) for weight in weights]
        + [
            pltpu.VMEM((rows, channels), BF16),
            pltpu.VMEM((halo_rows + rows, channels), F32),
            pltpu.VMEM((halo_rows, channels), BF16),
            pltpu.VMEM(map_shape, WIRE),
            pltpu.VMEM(map_shape, WIRE),
            pltpu.VMEM(map_shape, WIRE),
            pltpu.VMEM((groups,) + map_shape, WIRE),
            pltpu.VMEM((HEAD, width), F32),
            pltpu.VMEM((rows, width), F32),
            pltpu.VMEM((rows, width), F32),
            pltpu.VMEM((rows, channels), BF16),
            pltpu.VMEM((rows, width), BF16),
            pltpu.VMEM((n_tp, span, channels), BF16),
            pltpu.VMEM((n_tp, span, width), BF16),
            dma((13,)), dma((2,)), dma((2,)), dma((groups,)), dma((groups,)),
            dma((n_tp,)), dma((n_tp,)), dma((n_tp,)), dma((n_tp,)),
        ],
        compiler_params=pltpu.CompilerParams(
            collective_id=0, has_side_effects=True, vmem_limit_bytes=VMEM_LIMIT
        ),
    )(
        line(input_norm_gain), line(key_prenorm_gain), line(decay_offset_bias),
        depthwise_taps_weight, line(convolution_group_gain), line(convolution_group_shift),
        line(head_norm_gain), tokens, position_decay_shift, extra_log_decay, *weights,
    )


def solution(mesh):
    in_specs = (
        P("sp", None),
        P(),
        P(None, "tp"),
        P(None, "tp"),
        P(None, "tp"),
        P("tp"),
        P("tp"),
        P(None, "tp"),
        P(None, "tp"),
        P(None, "tp"),
        P(None, "tp"),
        P(None, "tp"),
        P(None, "tp"),
        P("tp"),
        P("tp"),
        P("sp", "tp"),
        P("sp", "tp"),
        P("tp"),
        P(),
        P(),
    )
    body = functools.partial(local, mesh.shape["sp"], mesh.shape["tp"])
    return jax.shard_map(
        body, mesh=mesh, in_specs=in_specs, out_specs=P(("sp", "tp"), None), check_vma=False
    )
```

profile of v0, /device:TPU:0, one launch (start us, length us, event | category | flops | bytes accessed | tf_op | source)
XLA Modules:
  0.0 28.4 jit_solution(10822473628144250412)
XLA Ops:
  0.0 26.8 %layer.1 = bf16[64,2048]{1,0:T(8,128)(2,1)} custom-call(f32[1,2048]{1,0:T(1,128)} %bitcast.6, f32[1,256]{1,0:T(1,128)} %bitcast.7, f32[1,256]{1,0:T(1,128)} %bitcast.8, f32[31,128]{1,0:T(8,128)} %taps.1, f32[1,128]{1,0:T(1,128)} %bitcast.10, f32[1,128]{1,0:T(1,128)} %bitcast.11, f32[1,256]{1,0:T(1,128)} %bitcast.9, bf16[256,2048]{1,0:T(8,128)(2,1)} %tok_hbm.1, ...), custom_call_target="tpu_custom_call" | custom-call | tf_op jit(solution)/shard_map/layer/pallas_call | solution.py:438
  26.8 1.7 %copy.22 = bf16[64,2048]{1,0:T(8,128)(2,1)} copy(bf16[64,2048]{1,0:T(8,128)(2,1)} %layer.1) | data formatting | bytes 524288
where the time goes:
time: 28.6 us; the launch traced here: 28.4 us
  Pallas kernels  26.8 us (94%)
  local copies, waits for them, and re-layouts  1.67 us (6%)
    pallas_call x1, Pallas kernels, local(): pl.pallas_call(functools.partial(layer_kernel, n_sp, n_tp), name='layer',...  26.8 us
    unnamed x1, local copies, waits for them, and re-layouts  1.67 us

commit v1 on v0

--- a/solution.py
+++ b/solution.py
@@ -88,25 +88,36 @@
 
 def layer_kernel(
     n_sp, n_tp,
-    gain, kgain, bias, taps, ggain, gshift, hgain,
+    gain_hbm, kgain_hbm, bias_hbm, taps_hbm, ggain_hbm, gshift_hbm, hgain_hbm,
     tok_hbm, shift_hbm, extra_hbm, wcv, wcg, wk, wr, wd, we, wv, wg, wco, wao,
     out,
+    gain, kgain, bias, taps, ggain, gshift, hgain,
     tok, shift, extra, cv_buf, cg_buf, k_buf, r_buf, d_buf, e_buf, v_buf, g_buf, co_buf, ao_buf,
     conv_in, extended, halo, own_map, partner_map, pair_map, maps, state,
     local_read, carried, conv_out, mix_out, conv_slots, mix_slots,
     weight_sem, halo_sem, pair_sem, map_send, map_recv, conv_send, conv_recv, mix_send, mix_recv,
 ):
     sp, tp = lax.axis_index("sp"), lax.axis_index("tp")
-    order = (
-        (tok_hbm, tok), (wk, k_buf), (we, e_buf), (shift_hbm, shift), (extra_hbm, extra),
-        (wd, d_buf), (wv, v_buf), (wcv, cv_buf), (wcg, cg_buf),
-        (wr, r_buf), (wg, g_buf), (wco, co_buf), (wao, ao_buf),
-    )
-    copies = []
-    for index, (source, buffer) in enumerate(order):
-        copy = pltpu.make_async_copy(source, buffer, weight_sem.at[index])
-        copy.start()
-        copies.append(copy)
+    half = tok_hbm.shape[0] // 2
+    order = dict(
+        gain=(gain_hbm, gain),
+        tok0=(tok_hbm.at[pl.ds(0, half)], tok.at[pl.ds(0, half)]),
+        tok1=(tok_hbm.at[pl.ds(half, half)], tok.at[pl.ds(half, half)]),
+        k=(wk, k_buf), e=(we, e_buf), kgain=(kgain_hbm, kgain), bias=(bias_hbm, bias),
+        d=(wd, d_buf), v=(wv, v_buf), shift=(shift_hbm, shift), extra=(extra_hbm, extra),
+        cv=(wcv, cv_buf), cg=(wcg, cg_buf), r=(wr, r_buf), g=(wg, g_buf),
+        taps=(taps_hbm, taps), ggain=(ggain_hbm, ggain), gshift=(gshift_hbm, gshift),
+        hgain=(hgain_hbm, hgain), co=(wco, co_buf), ao=(wao, ao_buf),
+    )
+    copies = {}
+    for index, (key, (source, buffer)) in enumerate(order.items()):
+        copies[key] = pltpu.make_async_copy(source, buffer, weight_sem.at[index])
+        copies[key].start()
+
+    def arrive(*keys):
+        for key in keys:
+            copies[key].wait()
+
     barrier = pltpu.get_barrier_semaphore()
     for step in range(1, n_sp):
         pl.semaphore_signal(
@@ -125,24 +136,30 @@
     groups = n_sp // 2
     group, parity = sp // 2, lax.rem(sp, 2)
     first_member = parity == 0
-    copies[0].wait()
-    x = tok[...].astype(F32)
-    normed = (
-        x * lax.rsqrt(jnp.mean(x * x, axis=-1, keepdims=True) + NORM_EPS) * gain[...]
-    ).astype(BF16)
-
-    def project(index):
-        copies[index].wait()
-        return dot(normed, order[index][1][...]).astype(BF16).astype(F32)
-
-    key_all = project(1)
+    halves = []
+    arrive("gain")
+    for index in range(2):
+        arrive("tok" + str(index))
+        x = tok[index * half:(index + 1) * half].astype(F32)
+        halves.append(
+            (
+                x * lax.rsqrt(jnp.mean(x * x, axis=-1, keepdims=True) + NORM_EPS) * gain[...]
+            ).astype(BF16)
+        )
+    normed = jnp.concatenate(halves, axis=0)
+
+    def kept(x):
+        return x.astype(BF16).astype(F32)
+
+    arrive("k", "e", "kgain")
+    key_all, rate = kept(dot(normed, k_buf[...])), kept(dot(normed, e_buf[...]))
+    arrive("d", "v", "bias", "shift", "extra")
+    slope, value = kept(dot(normed, d_buf[...])), kept(dot(normed, v_buf[...]))
     ones = jnp.where(head_blocks(width), 1.0, 0.0).astype(BF16)
     unit = key_all * kgain[...]
     unit = unit * lax.rsqrt(mm_left(unit * unit, ones) + KEY_EPS)
-    erase = unit * jax.nn.sigmoid(project(2))
-    copies[3].wait()
-    copies[4].wait()
-    logits = project(5) + bias[...] + shift[...]
+    erase = unit * jax.nn.sigmoid(rate)
+    logits = slope + bias[...] + shift[...]
     decay = jax.nn.sigmoid(logits) * (-0.6065306597126334) + extra[...]
     row, col = iota2(PAIR, PAIR)
     same = (row // CHUNK) == (col // CHUNK)
@@ -174,7 +191,6 @@
     keep = jnp.exp(final - cum)
     kept_erase = erase * keep
     kept_key = key_all * keep
-    value = project(6)
 
     units = [(h, p) for h in range(heads) for p in range(pairs)]
 
@@ -246,8 +262,10 @@
     )
     pair_copy.start()
 
-    conv_value = project(7)
-    conv_rows = (conv_value * jax.nn.sigmoid(project(8))).astype(BF16)
+    arrive("cv", "cg")
+    both = jnp.concatenate([cv_buf[...], cg_buf[...]], axis=1)
+    pair = kept(jnp.concatenate([dot(part, both) for part in halves], axis=0))
+    conv_rows = (pair[:, :channels] * jax.nn.sigmoid(pair[:, channels:])).astype(BF16)
     conv_in[...] = conv_rows
     halo_copy = pltpu.make_async_remote_copy(
         src_ref=conv_in.at[pl.ds(rows - halo_rows, halo_rows)], dst_ref=halo,
@@ -266,7 +284,9 @@
         trans = block_diagonal(block[HEAD:], width)
         return mm(carry, trans, "enter")
 
-    receptance = project(9)
+    arrive("r", "g", "hgain")
+    receptance, gate = kept(dot(normed, r_buf[...])), kept(dot(normed, g_buf[...]))
+    gate = jax.nn.sigmoid(gate) * hgain[...]
     left_read = receptance * jnp.exp(cum - mid)
     query_read = receptance * jnp.exp(cum)
 
@@ -299,6 +319,7 @@
     def _():
         extended[:halo_rows, :] = jnp.zeros((halo_rows, channels), F32)
 
+    arrive("taps", "ggain", "gshift")
     tap_count = taps.shape[0]
     total = jnp.zeros((rows, channels), F32)
     for offset in range(tap_count):
@@ -355,7 +376,6 @@
                 ) + mm(read[:, HEAD:], prior, "carry", NT)
             local_read[start:start + CHUNK, lanes] = read[:, :HEAD]
             carried[start:start + CHUNK, lanes] = read[:, HEAD:]
-    gate = jax.nn.sigmoid(project(10)) * hgain[...]
 
     own = pl.multiple_of(tp * span, span)
 
@@ -371,7 +391,7 @@
             )
         return result
 
-    copies[11].wait()
+    arrive("co")
     result = gather(
         jnp.zeros(out.shape, F32), conv_out, conv_slots, conv_copies, co_buf, channels
     )
@@ -392,7 +412,7 @@
     scaled = centred * lax.rsqrt(mm_left(centred * centred, head_means) + HEAD_EPS)
     mix_out[...] = (scaled * gate).astype(BF16)
     mix_copies = spread(mix_out, mix_slots, mix_send, mix_recv)
-    copies[12].wait()
+    arrive("ao")
     result = gather(result, mix_out, mix_slots, mix_copies, ao_buf, width)
     out[...] = result.astype(BF16)
     for copy in conv_copies + mix_copies:
@@ -425,6 +445,11 @@
     def line(values):
         return values.reshape(1, -1)
 
+    smalls = (
+        line(input_norm_gain), line(key_prenorm_gain), line(decay_offset_bias),
+        depthwise_taps_weight, line(convolution_group_gain), line(convolution_group_shift),
+        line(head_norm_gain),
+    )
     weights = (
         convolution_value_weight, convolution_gate_weight, key_weight, receptance_weight,
         decay_weight, correction_rate_weight, value_weight, output_gate_weight,
@@ -438,10 +463,11 @@
     return pl.pallas_call(
         functools.partial(layer_kernel, n_sp, n_tp),
         name="layer",
-        out_shape=jax.ShapeDtypeStruct((span, model), BF16),
-        in_specs=[vmem] * 7 + [anywhere] * 13,
+        out_shape=pltpu.VMEM((span, model), BF16),
+        in_specs=[anywhere] * 20,
         out_specs=vmem,
-        scratch_shapes=[
+        scratch_shapes=[pltpu.VMEM(small.shape, F32) for small in smalls]
+        + [
             pltpu.VMEM(tokens.shape, BF16),
             pltpu.VMEM(position_decay_shift.shape, F32),
             pltpu.VMEM(extra_log_decay.shape, F32),
@@ -462,16 +488,14 @@
             pltpu.VMEM((rows, width), BF16),
             pltpu.VMEM((n_tp, span, channels), BF16),
             pltpu.VMEM((n_tp, span, width), BF16),
-            dma((13,)), dma((2,)), dma((2,)), dma((groups,)), dma((groups,)),
+            dma((21,)), dma((2,)), dma((2,)), dma((groups,)), dma((groups,)),
             dma((n_tp,)), dma((n_tp,)), dma((n_tp,)), dma((n_tp,)),
         ],
         compiler_params=pltpu.CompilerParams(
             collective_id=0, has_side_effects=True, vmem_limit_bytes=VMEM_LIMIT
         ),
     )(
-        line(input_norm_gain), line(key_prenorm_gain), line(decay_offset_bias),
-        depthwise_taps_weight, line(convolution_group_gain), line(convolution_group_shift),
-        line(head_norm_gain), tokens, position_decay_shift, extra_log_decay, *weights,
+        *smalls, tokens, position_decay_shift, extra_log_decay, *weights,
     )
 
 

time: 28.6 us -> 24.5 us (0.86)
  the two profiles are of different devices: /device:TPU:0 before, /device:TPU:25 now
where the time goes in v1:
time: 24.5 us; the launch traced here: 24.3 us
  Pallas kernels  23.6 us (96%)
  local copies, waits for them, and re-layouts  0.71 us (3%)
    pallas_call x1, Pallas kernels, local(): pl.pallas_call(functools.partial(layer_kernel, n_sp, n_tp), name='layer',...  23.6 us
    unnamed x1, local copies, waits for them, and re-layouts  0.71 us

profile of v1, /device:TPU:25, one launch (start us, length us, event | category | flops | bytes accessed | tf_op | source)
XLA Modules:
  0.0 24.3 jit_solution(12423808511054750642)
XLA Ops:
  0.0 23.6 %layer.1 = bf16[64,2048]{1,0:T(8,128)(2,1)S(1)} custom-call(f32[1,2048]{1,0:T(1,128)} %bitcast.6, f32[1,256]{1,0:T(1,128)} %bitcast.7, f32[1,256]{1,0:T(1,128)} %bitcast.8, f32[31,128]{1,0:T(8,128)} %taps_hbm.1, f32[1,128]{1,0:T(1,128)} %bitcast.10, f32[1,128]{1,0:T(1,128)} %bitcast.11, f32[1,256]{1,0:T(1,128)} %bitcast.9, bf16[256,2048]{1,0:T(8,128)(2,1)} %tok_hbm.1, ...), custom_call_target="tpu_custom_call" | custom-call | tf_op jit(solution)/shard_map/layer/pallas_call | solution.py:463
  23.6 0.7 %copy.22 = bf16[64,2048]{1,0:T(8,128)(2,1)} copy(bf16[64,2048]{1,0:T(8,128)(2,1)S(1)} %layer.1) | data formatting | bytes 524288

commit v2 on v1

v2 whole, which is shorter than its diff:
```python
import functools

import jax
import jax.numpy as jnp
from jax import lax
from jax.experimental import pallas as pl
from jax.experimental.pallas import tpu as pltpu
from jax.sharding import PartitionSpec as P

HEAD = 64
CHUNK = 64
TOKEN_PARTS = 4
PAIR = 128

NORM_EPS = 1e-06
GROUP_EPS = 1e-05
HEAD_EPS = 0.00064
KEY_EPS = 1e-06
MESH = pl.DeviceIdType.MESH
WIRE = jnp.bfloat16
VMEM_LIMIT = 60 * 1024 * 1024
F32 = jnp.float32
BF16 = jnp.bfloat16

NN = (((1,), (0,)), ((), ()))
NT = (((1,), (1,)), ((), ()))
TN = (((0,), (0,)), ((), ()))


def parts(x, count):
    out = []
    for _ in range(count - 1):
        piece = x.astype(BF16)
        out.append(piece)
        x = x - piece.astype(F32)
    out.append(x.astype(BF16))
    return out


def dot(a, b, dims=NN):
    return lax.dot_general(a, b, dims, preferred_element_type=F32)


def mm_left(a, b, dims=NN, count=2):
    pieces = [dot(piece, b, dims) for piece in parts(a, count)]
    return functools.reduce(jnp.add, pieces)


def split(x):
    high = x.astype(BF16)
    return high, (x - high.astype(F32)).astype(BF16)


def concat(pieces, axis=0):
    return jnp.concatenate(pieces, axis=axis)


def iota2(rows, cols):
    return (
        lax.broadcasted_iota(jnp.int32, (rows, cols), 0),
        lax.broadcasted_iota(jnp.int32, (rows, cols), 1),
    )


def head_blocks(width):
    row, col = iota2(width, width)
    return (row // HEAD) == (col // HEAD)


def own_head(shape):
    row, col = iota2(*shape)
    return (row // HEAD) == ((col % PAIR) // HEAD)


def diagonal(x):
    lane = lax.broadcasted_iota(jnp.int32, x.shape, 1)
    zero = jnp.zeros_like(x)
    return concat([jnp.where(lane < HEAD, x, zero), jnp.where(lane < HEAD, zero, x)])


def spread_pair(x):
    return concat([diagonal(x[:, :PAIR]), diagonal(x[:, PAIR:])], axis=1)


def compose(later, earlier):
    high, low = split(later[:, PAIR:])
    early_high, early_low = split(earlier)
    both = dot(concat([high, low]), spread_pair(early_high))
    out = both[:HEAD] + both[HEAD:] + dot(high, spread_pair(early_low))
    return concat([out[:, :PAIR] + later[:, :PAIR], out[:, PAIR:]], axis=1)


def layer_kernel(
    n_sp, n_tp,
    gain_hbm, kgain_hbm, bias_hbm, taps_hbm, ggain_hbm, gshift_hbm, hgain_hbm,
    tok_hbm, shift_hbm, extra_hbm, wcv, wcg, wk, wr, wd, we, wv, wg, wco, wao,
    out,
    gain, kgain, bias, taps, ggain, gshift, hgain,
    tok, shift, extra, cv_buf, cg_buf, k_buf, r_buf, d_buf, e_buf, v_buf, g_buf, co_buf, ao_buf,
    conv_in, extended, halo, own_map, partner_map, pair_map, maps, windows, state, reach,
    local_read, carried, conv_out, mix_out, conv_slots, mix_slots,
    weight_sem, halo_sem, pair_sem, map_send, map_recv, conv_send, conv_recv, mix_send, mix_recv,
):
    sp, tp = lax.axis_index("sp"), lax.axis_index("tp")
    part = tok_hbm.shape[0] // TOKEN_PARTS
    order = dict(gain=(gain_hbm, gain))
    for index in range(TOKEN_PARTS):
        span = pl.ds(index * part, part)
        order["tok" + str(index)] = (tok_hbm.at[span], tok.at[span])
    order.update(
        k=(wk, k_buf), e=(we, e_buf), kgain=(kgain_hbm, kgain),
        d=(wd, d_buf), v=(wv, v_buf), bias=(bias_hbm, bias),
        shift=(shift_hbm, shift), extra=(extra_hbm, extra),
        cv=(wcv, cv_buf), cg=(wcg, cg_buf), r=(wr, r_buf), g=(wg, g_buf),
        taps=(taps_hbm, taps), ggain=(ggain_hbm, ggain), gshift=(gshift_hbm, gshift),
        hgain=(hgain_hbm, hgain), co=(wco, co_buf), ao=(wao, ao_buf),
    )
    copies = {}
    for index, (key, (source, buffer)) in enumerate(order.items()):
        copies[key] = pltpu.make_async_copy(source, buffer, weight_sem.at[index])

    def begin(*keys):
        for key in keys:
            copies[key].start()

    def arrive(*keys):
        for key in keys:
            copies[key].wait()

    token_keys = ["tok" + str(index) for index in range(TOKEN_PARTS)]
    begin("gain", *token_keys, "k", "e", "kgain", "d", "v", "bias", "shift", "extra")
    barrier = pltpu.get_barrier_semaphore()
    for step in range(1, n_sp):
        pl.semaphore_signal(
            barrier, inc=1, device_id=(lax.rem(sp + step, n_sp), tp), device_id_type=MESH
        )
    for step in range(1, n_tp):
        pl.semaphore_signal(
            barrier, inc=1, device_id=(sp, lax.rem(tp + step, n_tp)), device_id_type=MESH
        )
    rows = tok.shape[0]
    channels = conv_in.shape[1]
    width = local_read.shape[1]
    heads = width // HEAD
    pairs = rows // PAIR
    halo_rows = halo.shape[0]
    groups = n_sp // 2
    group, parity = sp // 2, lax.rem(sp, 2)
    first_member = parity == 0
    quarters = []
    arrive("gain")
    for index, key in enumerate(token_keys):
        arrive(key)
        x = tok[index * part:(index + 1) * part].astype(F32)
        quarters.append(
            (
                x * lax.rsqrt(jnp.mean(x * x, axis=-1, keepdims=True) + NORM_EPS) * gain[...]
            ).astype(BF16)
        )
    begin("cv", "cg", "r", "g", "taps", "ggain", "gshift", "hgain")
    middle_part = TOKEN_PARTS // 2
    halves = [concat(quarters[:middle_part]), concat(quarters[middle_part:])]
    normed = concat(halves)

    def kept(x):
        return x.astype(BF16).astype(F32)

    arrive("k", "e", "kgain")
    key_all, rate = kept(dot(normed, k_buf[...])), kept(dot(normed, e_buf[...]))
    arrive("d", "v", "bias", "shift", "extra")
    begin("co", "ao")
    slope = kept(dot(normed, d_buf[...]))
    value = dot(normed, v_buf[...]).astype(BF16)
    same_head = head_blocks(width)
    ones = jnp.where(same_head, 1.0, 0.0).astype(BF16)
    row, col = iota2(width, width)
    centre = (jnp.where(row == col, 1.0, 0.0) - jnp.where(same_head, 1.0 / HEAD, 0.0)).astype(BF16)
    unit = key_all * kgain[...]
    unit = unit * lax.rsqrt(dot((unit * unit).astype(BF16), ones) + KEY_EPS)
    erase = -(unit * jax.nn.sigmoid(rate))
    value_high, value_low = split(dot(value, centre))
    logits = slope + bias[...] + shift[...]
    decay = jax.nn.sigmoid(logits) * (-0.6065306597126334) + extra[...]
    row, col = iota2(PAIR, 2 * PAIR)
    col = col % PAIR
    tri = jnp.where(((row // CHUNK) == (col // CHUNK)) & (row >= col), 1.0, 0.0).astype(BF16)
    cum = concat(
        [dot(tri, concat(split(decay[p:p + PAIR]))) for p in range(0, rows, PAIR)]
    )
    chunks = rows // CHUNK
    groups_of = width // PAIR

    def by_chunk(row_of):
        return concat(
            [jnp.broadcast_to(row_of(c), (CHUNK, width)) for c in range(0, rows, CHUNK)]
        )

    def middle(c):
        return cum[c + CHUNK // 2 - 1:c + CHUNK // 2]

    def last(c):
        return cum[c + CHUNK - 1:c + CHUNK]

    mid = by_chunk(middle)
    from_start = by_chunk(lambda c: jnp.exp(middle(c)))
    to_end = by_chunk(lambda c: jnp.exp(last(c) - middle(c)))
    up = jnp.exp(mid - cum)
    left_unit = unit * jnp.exp(cum - decay - mid)
    query_unit = (left_unit * from_start).astype(BF16)
    left_unit = left_unit.astype(BF16)
    right_erase, right_key = erase * up, key_all * up
    kept_erase, kept_key = (right_erase * to_end).astype(BF16), (right_key * to_end).astype(BF16)
    right_erase, right_key = right_erase.astype(BF16), right_key.astype(BF16)
    units = [(c, g) for c in range(chunks) for g in range(groups_of)]

    def piece(values, unit_index):
        c, g = unit_index
        return values[c * CHUNK:(c + 1) * CHUNK, g * PAIR:(g + 1) * PAIR]

    row, col = iota2(CHUNK, PAIR)
    col = col % CHUNK
    strict, inclusive = row > col, row >= col
    eye = jnp.where(row == col, 1.0, 0.0)
    rights = [
        concat([diagonal(piece(right_erase, u)), diagonal(piece(right_key, u))]) for u in units
    ]
    products = [dot(piece(left_unit, u), right, NT) for u, right in zip(units, rights)]
    lower = [jnp.where(strict, product[:, :PAIR], 0.0) for product in products]
    mixes = [jnp.where(strict, product[:, PAIR:], 0.0).astype(BF16) for product in products]
    value_diagonals = [
        concat([diagonal(piece(value_high, u)), diagonal(piece(value_low, u))]) for u in units
    ]
    mixed = [
        dot(concat([mix, mix], axis=1), both) for mix, both in zip(mixes, value_diagonals)
    ]
    first = strict & ((row // 2) == (col // 2))
    inverse = [eye + jnp.where(first, low, 0.0) for low in lower]
    size = 2
    while size < CHUNK:
        level = ((row // (2 * size)) == (col // (2 * size))) & ((row // size) > (col // size))
        narrow = [inv.astype(BF16) for inv in inverse]
        inner = [
            dot(jnp.where(level, low, 0.0).astype(BF16), diagonal(inv))
            for low, inv in zip(lower, narrow)
        ]
        inverse = [
            inv + dot(left, diagonal(step.astype(BF16)))
            for inv, left, step in zip(inverse, narrow, inner)
        ]
        size *= 2
    solved = [
        dot(
            inv.astype(BF16),
            concat([diagonal(mix.astype(BF16)), diagonal(piece(query_unit, u))], axis=1),
        ).astype(BF16)
        for inv, mix, u in zip(inverse, mixed, units)
    ]
    nothing = jnp.zeros((CHUNK, PAIR), BF16)
    lane = lax.broadcasted_iota(jnp.int32, (HEAD, 2 * PAIR), 1)
    first_head = (lane % PAIR) < HEAD
    blocks = {}
    for index, u in enumerate(units):
        c, g = u
        left = concat([piece(kept_erase, u), piece(kept_key, u), piece(kept_key, u)])
        right = concat(
            [
                solved[index],
                concat([piece(value_high, u), nothing], axis=1),
                concat([piece(value_low, u), nothing], axis=1),
            ]
        )
        product = dot(left, right, TN)
        product = jnp.where(first_head, product[:HEAD], product[HEAD:])
        stay = jnp.exp(last(c * CHUNK)[:, g * PAIR:(g + 1) * PAIR])
        blocks[u] = concat([product[:, :PAIR], product[:, PAIR:] + eye * stay], axis=1)
    spans = {}
    for c in range(chunks):
        for g in range(groups_of):
            spans[c, c + 1, g] = blocks[c, g]
    size = 1
    while size < chunks:
        for c in range(0, chunks, 2 * size):
            for g in range(groups_of):
                spans[c, c + 2 * size, g] = compose(
                    spans[c + size, c + 2 * size, g], spans[c, c + size, g]
                )
        size *= 2
    totals = [spans[0, chunks, g] for g in range(groups_of)]
    own_total = concat(
        [
            concat([totals[g][:, :PAIR] for g in range(groups_of)], axis=1),
            concat([totals[g][:, PAIR:] for g in range(groups_of)], axis=1),
        ]
    ).astype(WIRE)
    own_map[...] = own_total

    pl.semaphore_wait(barrier, n_sp + n_tp - 2)
    pair_copy = pltpu.make_async_remote_copy(
        src_ref=own_map, dst_ref=partner_map, send_sem=pair_sem.at[0], recv_sem=pair_sem.at[1],
        device_id=(sp + 1 - 2 * parity, tp), device_id_type=MESH,
    )
    pair_copy.start()

    arrive("cv", "cg")
    both = concat([cv_buf[...], cg_buf[...]], axis=1)
    conv_pair = kept(concat([dot(part, both) for part in halves]))
    conv_rows = (
        conv_pair[:, :channels] * jax.nn.sigmoid(conv_pair[:, channels:])
    ).astype(BF16)
    conv_in[...] = conv_rows
    halo_copy = pltpu.make_async_remote_copy(
        src_ref=conv_in.at[pl.ds(rows - halo_rows, halo_rows)], dst_ref=halo,
        send_sem=halo_sem.at[0], recv_sem=halo_sem.at[1],
        device_id=(sp + 1, tp), device_id_type=MESH,
    )
    has_next = sp + 1 < n_sp

    @pl.when(has_next)
    def _():
        halo_copy.start()

    extended[halo_rows:, :] = conv_rows.astype(F32)

    arrive("r", "g", "hgain")
    receptance, gate = kept(dot(normed, r_buf[...])), kept(dot(normed, g_buf[...]))
    left_read = receptance * jnp.exp(cum - mid)
    query_read = left_read * from_start
    left_read = left_read.astype(BF16)
    gate = jax.nn.sigmoid(gate) * hgain[...]
    zeros = jnp.zeros((PAIR, PAIR), BF16)
    products = [dot(piece(left_read, u), right, NT) for u, right in zip(units, rights)]
    reads = []
    for product, end, both, u in zip(products, solved, value_diagonals, units):
        keys = jnp.where(inclusive, product[:, PAIR:], 0.0).astype(BF16)
        mix = concat(
            [jnp.where(inclusive, product[:, :PAIR], 0.0).astype(BF16), keys, keys], axis=1
        )
        stacked = concat(
            [spread_pair(end), concat([both, concat([zeros, zeros])], axis=1)]
        )
        reads.append(dot(mix, stacked))
    priors = {}
    for c in range(1, chunks):
        start, size = 0, chunks // 2
        while start < c:
            while start + size > c:
                size //= 2
            for g in range(groups_of):
                block = spans[start, start + size, g]
                priors[c, g] = block if start == 0 else compose(block, priors[c, g])
            start += size
    for index, u in enumerate(units):
        c, g = u
        near, far = reads[index][:, :PAIR], reads[index][:, PAIR:] + piece(query_read, u)
        if c > 0:
            moved = dot(far.astype(BF16), spread_pair(priors[u].astype(BF16)))
            near, far = near + moved[:, :PAIR], moved[:, PAIR:]
        span = slice(c * CHUNK, (c + 1) * CHUNK)
        lanes = slice(g * PAIR, (g + 1) * PAIR)
        local_read[span, lanes] = near
        carried[span, lanes] = far.astype(BF16)

    def by_pair(x):
        return [x[:, g * PAIR:(g + 1) * PAIR] for g in range(groups_of)]

    def chain(held, move):
        out = []
        for state_part, move_part in zip(by_pair(held), by_pair(move)):
            right = concat([diagonal(piece_of) for piece_of in split(state_part)])
            out.append(dot(concat([move_part, move_part], axis=1), right))
        return concat(out, axis=1)

    pair_copy.wait()
    mine, theirs = own_total.astype(F32), partner_map[...].astype(F32)
    early = jnp.where(first_member, mine, theirs).astype(WIRE)
    late = jnp.where(first_member, theirs, mine).astype(WIRE)
    joined = [
        dot(move, spread_pair(concat([add, keep], axis=1)))
        for move, add, keep in zip(by_pair(late[HEAD:]), by_pair(early[:HEAD]), by_pair(early[HEAD:]))
    ]
    pair_map[:HEAD] = (
        concat([part[:, :PAIR] for part in joined], axis=1) + late[:HEAD].astype(F32)
    ).astype(WIRE)
    pair_map[HEAD:] = concat([part[:, PAIR:] for part in joined], axis=1).astype(WIRE)

    hops = []
    while 2 ** len(hops) < groups:
        hops.append(2 ** len(hops))

    def hop(source, k, side):
        span_of = pl.ds(side * HEAD, HEAD)
        return pltpu.make_async_remote_copy(
            src_ref=source.at[span_of], dst_ref=maps.at[k, span_of],
            send_sem=map_send.at[2 * k + side], recv_sem=map_recv.at[2 * k + side],
            device_id=(sp + 2 * hops[k], tp), device_id_type=MESH,
        )

    sends = []
    for k, ahead in enumerate(hops):
        reached = group + ahead < groups
        if k == 0:
            sends.append((k, reached, pair_map, 0))
            sends.append((k, reached & (group >= 1), pair_map, 1))
        else:
            sends.append((0, group == 0, pair_map, 0, k))
            sends.append((k, reached & (group >= 1), windows.at[k], 0))
            if 2 * ahead < groups:
                sends.append((k, reached & (group >= ahead), windows.at[k], 1))

    def send_step(step):
        for when, allowed, source, side, *target in sends:
            if when == step:
                @pl.when(allowed)
                def _():
                    hop(source, target[0] if target else step, side).start()

    if hops:
        send_step(0)

    @pl.when(sp > 0)
    def _():
        halo_copy.wait_recv()
        extended[:halo_rows, :] = halo[...].astype(F32)

    @pl.when(sp == 0)
    def _():
        extended[:halo_rows, :] = jnp.zeros((halo_rows, channels), F32)

    arrive("taps", "ggain", "gshift")
    tap_count = taps.shape[0]
    total = jnp.zeros((rows, channels), F32)
    for offset in range(tap_count):
        begin = halo_rows - tap_count + 1 + offset
        total = total + taps[offset:offset + 1, :] * extended[begin:begin + rows, :]
    means = jnp.where(head_blocks(channels), 1.0 / HEAD, 0.0).astype(BF16)
    centred = total - mm_left(total, means)
    scaled = centred * lax.rsqrt(mm_left(centred * centred, means) + GROUP_EPS)
    conv_out[...] = jax.nn.silu(scaled * ggain[...] + gshift[...]).astype(BF16)

    span = rows // n_tp

    def spread(source, slots, send, recv):
        started = []
        for step in range(1, n_tp):
            target = lax.rem(tp + step, n_tp)
            begin = pl.multiple_of(target * span, span)
            copy = pltpu.make_async_remote_copy(
                src_ref=source.at[pl.ds(begin, span)], dst_ref=slots.at[step],
                send_sem=send.at[step], recv_sem=recv.at[step],
                device_id=(sp, target), device_id_type=MESH,
            )
            copy.start()
            started.append(copy)
        return started

    conv_copies = spread(conv_out, conv_slots, conv_send, conv_recv)

    own = pl.multiple_of(tp * span, span)

    def gather(result, source, slots, arriving, weight, depth):
        result = result + dot(
            source[pl.ds(own, span)], weight[pl.ds(pl.multiple_of(tp * depth, depth), depth)]
        )
        for step in range(1, n_tp):
            arriving[step - 1].wait_recv()
            begin = lax.rem(tp - step + n_tp, n_tp) * depth
            result = result + dot(
                slots[step], weight[pl.ds(pl.multiple_of(begin, depth), depth)]
            )
        return result

    state[...] = jnp.zeros_like(state)
    for k, ahead in enumerate(hops):
        @pl.when(group >= ahead)
        def _():
            hop(pair_map, k, 0).wait_recv()
            arrived = maps[k, :HEAD].astype(F32)
            state[...] = arrived if k == 0 else chain(arrived, reach[...]) + state[...]

        if 2 * ahead < groups:
            @pl.when(group >= 2 * ahead)
            def _():
                hop(pair_map, k, 1).wait_recv()
                further = maps[k, HEAD:]
                if k > 0:
                    further = chain(further.astype(F32), reach[...]).astype(WIRE)
                reach[...] = further

            following = 2 * ahead

            @pl.when((group >= 1) & (group + following < groups))
            def _():
                windows[k + 1, :HEAD] = (
                    chain(state[...], pair_map[HEAD:]) + pair_map[:HEAD].astype(F32)
                ).astype(WIRE)

            if 2 * following < groups:
                @pl.when((group >= following) & (group + following < groups))
                def _():
                    windows[k + 1, HEAD:] = chain(
                        reach[...].astype(F32), pair_map[HEAD:]
                    ).astype(WIRE)

            send_step(k + 1)

    behind = chain(state[...], early[HEAD:]) + early[:HEAD].astype(F32)
    entering = jnp.where(first_member, state[...], behind).astype(BF16)
    centred = local_read[...] + concat(
        [
            dot(carried[:, g * PAIR:(g + 1) * PAIR], diagonal(part))
            for g, part in enumerate(by_pair(entering))
        ],
        axis=1,
    )
    head_means = jnp.where(same_head, 1.0 / HEAD, 0.0).astype(BF16)
    scaled = centred * lax.rsqrt(dot((centred * centred).astype(BF16), head_means) + HEAD_EPS)
    mix_out[...] = (scaled * gate).astype(BF16)
    mix_copies = spread(mix_out, mix_slots, mix_send, mix_recv)
    arrive("co")
    result = gather(
        jnp.zeros(out.shape, F32), conv_out, conv_slots, conv_copies, co_buf, channels
    )

    arrive("ao")
    result = gather(result, mix_out, mix_slots, mix_copies, ao_buf, width)
    out[...] = result.astype(BF16)
    for copy in conv_copies + mix_copies:
        copy.wait_send()

    @pl.when(has_next)
    def _():
        halo_copy.wait_send()

    for when, allowed, source, side, *target in sends:
        @pl.when(allowed)
        def _():
            hop(source, target[0] if target else when, side).wait_send()


def local(
    n_sp, n_tp,
    tokens, input_norm_gain, convolution_value_weight, convolution_gate_weight,
    depthwise_taps_weight, convolution_group_gain, convolution_group_shift,
    receptance_weight, key_weight, value_weight, decay_weight, correction_rate_weight,
    output_gate_weight, key_prenorm_gain, decay_offset_bias, position_decay_shift,
    extra_log_decay, head_norm_gain, convolution_output_weight, attention_output_weight,
):
    rows, model = tokens.shape
    channels = convolution_value_weight.shape[1]
    width = key_weight.shape[1]
    vmem = pl.BlockSpec(memory_space=pltpu.VMEM)
    anywhere = pl.BlockSpec(memory_space=pl.ANY)

    def line(values):
        return values.reshape(1, -1)

    smalls = (
        line(input_norm_gain), line(key_prenorm_gain), line(decay_offset_bias),
        depthwise_taps_weight, line(convolution_group_gain), line(convolution_group_shift),
        line(head_norm_gain),
    )
    weights = (
        convolution_value_weight, convolution_gate_weight, key_weight, receptance_weight,
        decay_weight, correction_rate_weight, value_weight, output_gate_weight,
        convolution_output_weight, attention_output_weight,
    )
    span = rows // n_tp
    halo_rows = -(-(depthwise_taps_weight.shape[0] - 1) // 16) * 16
    hop_count = max(1, (n_sp // 2 - 1).bit_length())
    dma = pltpu.SemaphoreType.DMA
    map_shape = (2 * HEAD, width)
    return pl.pallas_call(
        functools.partial(layer_kernel, n_sp, n_tp),
        name="layer",
        out_shape=pltpu.VMEM((span, model), BF16),
        in_specs=[anywhere] * 20,
        out_specs=vmem,
        scratch_shapes=[pltpu.VMEM(small.shape, F32) for small in smalls]
        + [
            pltpu.VMEM(tokens.shape, BF16),
            pltpu.VMEM(position_decay_shift.shape, F32),
            pltpu.VMEM(extra_log_decay.shape, F32),
        ]
        + [pltpu.VMEM(weight.shape, BF16) for weight in weights]
        + [
            pltpu.VMEM((rows, channels), BF16),
            pltpu.VMEM((halo_rows + rows, channels), F32),
            pltpu.VMEM((halo_rows, channels), BF16),
            pltpu.VMEM(map_shape, WIRE),
            pltpu.VMEM(map_shape, WIRE),
            pltpu.VMEM(map_shape, WIRE),
            pltpu.VMEM((hop_count,) + map_shape, WIRE),
            pltpu.VMEM((hop_count,) + map_shape, WIRE),
            pltpu.VMEM((HEAD, width), F32),
            pltpu.VMEM((HEAD, width), WIRE),
            pltpu.VMEM((rows, width), F32),
            pltpu.VMEM((rows, width), BF16),
            pltpu.VMEM((rows, channels), BF16),
            pltpu.VMEM((rows, width), BF16),
            pltpu.VMEM((n_tp, span, channels), BF16),
            pltpu.VMEM((n_tp, span, width), BF16),
            dma((24,)), dma((2,)), dma((2,)), dma((2 * hop_count,)), dma((2 * hop_count,)),
            dma((n_tp,)), dma((n_tp,)), dma((n_tp,)), dma((n_tp,)),
        ],
        compiler_params=pltpu.CompilerParams(
            collective_id=0, has_side_effects=True, vmem_limit_bytes=VMEM_LIMIT
        ),
    )(
        *smalls, tokens, position_decay_shift, extra_log_decay, *weights,
    )


def solution(mesh):
    in_specs = (
        P("sp", None),
        P(),
        P(None, "tp"),
        P(None, "tp"),
        P(None, "tp"),
        P("tp"),
        P("tp"),
        P(None, "tp"),
        P(None, "tp"),
        P(None, "tp"),
        P(None, "tp"),
        P(None, "tp"),
        P(None, "tp"),
        P("tp"),
        P("tp"),
        P("sp", "tp"),
        P("sp", "tp"),
        P("tp"),
        P(),
        P(),
    )
    body = functools.partial(local, mesh.shape["sp"], mesh.shape["tp"])
    return jax.shard_map(
        body, mesh=mesh, in_specs=in_specs, out_specs=P(("sp", "tp"), None), check_vma=False
    )
```

time: 24.5 us -> 20.9 us (0.85)
  Pallas kernels: 23.6 us -> 20 us
    pallas_call x1, Pallas kernels: 23.6 us -> 20 us  [local(): pl.pallas_call(functools.partial(layer_kernel, n_sp, n_tp), name='layer',...]
where the time goes in v2:
time: 20.9 us; the launch traced here: 20.7 us
  Pallas kernels  20 us (96%)
  local copies, waits for them, and re-layouts  0.71 us (3%)
    pallas_call x1, Pallas kernels, local(): pl.pallas_call(functools.partial(layer_kernel, n_sp, n_tp), name='layer',...  20 us
    unnamed x1, local copies, waits for them, and re-layouts  0.71 us

profile of v2, /device:TPU:25, one launch (start us, length us, event | category | flops | bytes accessed | tf_op | source)
XLA Modules:
  0.0 20.7 jit_solution(12011995318977062228)
XLA Ops:
  0.0 20.0 %layer.1 = bf16[64,2048]{1,0:T(8,128)(2,1)S(1)} custom-call(f32[1,2048]{1,0:T(1,128)} %bitcast.6, f32[1,256]{1,0:T(1,128)} %bitcast.7, f32[1,256]{1,0:T(1,128)} %bitcast.8, f32[31,128]{1,0:T(8,128)} %taps_hbm.1, f32[1,128]{1,0:T(1,128)} %bitcast.10, f32[1,128]{1,0:T(1,128)} %bitcast.11, f32[1,256]{1,0:T(1,128)} %bitcast.9, bf16[256,2048]{1,0:T(8,128)(2,1)} %tok_hbm.1, ...), custom_call_target="tpu_custom_call" | custom-call | tf_op jit(solution)/shard_map/layer/pallas_call | solution.py:572
  20.0 0.7 %copy.22 = bf16[64,2048]{1,0:T(8,128)(2,1)} copy(bf16[64,2048]{1,0:T(8,128)(2,1)S(1)} %layer.1) | data formatting | bytes 524288

commit v3 on v2

--- a/solution.py
+++ b/solution.py
@@ -9,7 +9,7 @@
 
 HEAD = 64
 CHUNK = 64
-TOKEN_PARTS = 4
+TOKEN_PARTS = 2
 PAIR = 128
 
 NORM_EPS = 1e-06
@@ -97,9 +97,9 @@
     out,
     gain, kgain, bias, taps, ggain, gshift, hgain,
     tok, shift, extra, cv_buf, cg_buf, k_buf, r_buf, d_buf, e_buf, v_buf, g_buf, co_buf, ao_buf,
-    conv_in, extended, halo, own_map, partner_map, pair_map, maps, windows, state, reach,
+    conv_in, extended, halo, own_map, partner_map, pair_map, early_map, maps, windows, state, reach, entered,
     local_read, carried, conv_out, mix_out, conv_slots, mix_slots,
-    weight_sem, halo_sem, pair_sem, map_send, map_recv, conv_send, conv_recv, mix_send, mix_recv,
+    weight_sem, halo_sem, pair_sem, map_send, map_recv, cross_send, conv_send, conv_recv, mix_send, mix_recv,
 ):
     sp, tp = lax.axis_index("sp"), lax.axis_index("tp")
     part = tok_hbm.shape[0] // TOKEN_PARTS
@@ -108,9 +108,8 @@
         span = pl.ds(index * part, part)
         order["tok" + str(index)] = (tok_hbm.at[span], tok.at[span])
     order.update(
-        k=(wk, k_buf), e=(we, e_buf), kgain=(kgain_hbm, kgain),
-        d=(wd, d_buf), v=(wv, v_buf), bias=(bias_hbm, bias),
-        shift=(shift_hbm, shift), extra=(extra_hbm, extra),
+        k=(wk, k_buf), kgain=(kgain_hbm, kgain), d=(wd, d_buf), bias=(bias_hbm, bias),
+        shift=(shift_hbm, shift), extra=(extra_hbm, extra), e=(we, e_buf), v=(wv, v_buf),
         cv=(wcv, cv_buf), cg=(wcg, cg_buf), r=(wr, r_buf), g=(wg, g_buf),
         taps=(taps_hbm, taps), ggain=(ggain_hbm, ggain), gshift=(gshift_hbm, gshift),
         hgain=(hgain_hbm, hgain), co=(wco, co_buf), ao=(wao, ao_buf),
@@ -128,7 +127,7 @@
             copies[key].wait()
 
     token_keys = ["tok" + str(index) for index in range(TOKEN_PARTS)]
-    begin("gain", *token_keys, "k", "e", "kgain", "d", "v", "bias", "shift", "extra")
+    begin("gain", *token_keys, "k", "kgain", "d", "bias", "shift", "extra", "e", "v")
     barrier = pltpu.get_barrier_semaphore()
     for step in range(1, n_sp):
         pl.semaphore_signal(
@@ -165,20 +164,18 @@
     def kept(x):
         return x.astype(BF16).astype(F32)
 
-    arrive("k", "e", "kgain")
-    key_all, rate = kept(dot(normed, k_buf[...])), kept(dot(normed, e_buf[...]))
-    arrive("d", "v", "bias", "shift", "extra")
+    def project(weight):
+        return concat([dot(half, weight[...]) for half in halves])
+
+    arrive("k", "d")
+    key_all, slope = kept(dot(normed, k_buf[...])), kept(dot(normed, d_buf[...]))
+    arrive("bias", "shift", "extra", "kgain", "e", "v")
     begin("co", "ao")
-    slope = kept(dot(normed, d_buf[...]))
-    value = dot(normed, v_buf[...]).astype(BF16)
+    rate = kept(project(e_buf))
     same_head = head_blocks(width)
     ones = jnp.where(same_head, 1.0, 0.0).astype(BF16)
     row, col = iota2(width, width)
     centre = (jnp.where(row == col, 1.0, 0.0) - jnp.where(same_head, 1.0 / HEAD, 0.0)).astype(BF16)
-    unit = key_all * kgain[...]
-    unit = unit * lax.rsqrt(dot((unit * unit).astype(BF16), ones) + KEY_EPS)
-    erase = -(unit * jax.nn.sigmoid(rate))
-    value_high, value_low = split(dot(value, centre))
     logits = slope + bias[...] + shift[...]
     decay = jax.nn.sigmoid(logits) * (-0.6065306597126334) + extra[...]
     row, col = iota2(PAIR, 2 * PAIR)
@@ -187,6 +184,11 @@
     cum = concat(
         [dot(tri, concat(split(decay[p:p + PAIR]))) for p in range(0, rows, PAIR)]
     )
+    unit = key_all * kgain[...]
+    unit = unit * lax.rsqrt(dot((unit * unit).astype(BF16), ones) + KEY_EPS)
+    value = project(v_buf).astype(BF16)
+    erase = -(unit * jax.nn.sigmoid(rate))
+    value_high, value_low = split(dot(value, centre))
     chunks = rows // CHUNK
     groups_of = width // PAIR
 
@@ -233,27 +235,44 @@
     mixed = [
         dot(concat([mix, mix], axis=1), both) for mix, both in zip(mixes, value_diagonals)
     ]
-    first = strict & ((row // 2) == (col // 2))
-    inverse = [eye + jnp.where(first, low, 0.0) for low in lower]
-    size = 2
-    while size < CHUNK:
-        level = ((row // (2 * size)) == (col // (2 * size))) & ((row // size) > (col // size))
-        narrow = [inv.astype(BF16) for inv in inverse]
-        inner = [
-            dot(jnp.where(level, low, 0.0).astype(BF16), diagonal(inv))
-            for low, inv in zip(lower, narrow)
-        ]
-        inverse = [
-            inv + dot(left, diagonal(step.astype(BF16)))
-            for inv, left, step in zip(inverse, narrow, inner)
-        ]
-        size *= 2
+    def within(size):
+        return (row // size) == (col // size)
+
+    def powers(left, right):
+        return dot(left, concat([diagonal(right), diagonal(left)], axis=1))
+
+    step = [jnp.where(within(4), low, 0.0) for low in lower]
+    inverse = [eye + s for s in step]
+    narrow = [s.astype(BF16) for s in step]
+    square = [dot(s, diagonal(s)).astype(BF16) for s in narrow]
+    inverse = [
+        inv + dot(s, diagonal(inv.astype(BF16))) for inv, s in zip(inverse, square)
+    ]
+    narrow = [inv.astype(BF16) for inv in inverse]
+    step = [
+        dot(inv, diagonal(jnp.where(within(16) & ~within(4), low, 0.0).astype(BF16))).astype(BF16)
+        for inv, low in zip(narrow, lower)
+    ]
+    both = [powers(s, inv) for s, inv in zip(step, narrow)]
+    inverse = [inv + pair[:, :PAIR] for inv, pair in zip(inverse, both)]
+    square = [pair[:, PAIR:].astype(BF16) for pair in both]
+    inverse = [
+        (inv + dot(s, diagonal(inv.astype(BF16)))).astype(BF16) for inv, s in zip(inverse, square)
+    ]
+    sides = [
+        spread_pair(concat([mix.astype(BF16), piece(query_unit, u)], axis=1))
+        for mix, u in zip(mixed, units)
+    ]
+    outer = [diagonal(jnp.where(within(16), 0.0, low).astype(BF16)) for low in lower]
+    step = [dot(inv, far).astype(BF16) for inv, far in zip(inverse, outer)]
+    solved = [dot(inv, side) for inv, side in zip(inverse, sides)]
+    square = [dot(s, diagonal(s)).astype(BF16) for s in step]
     solved = [
-        dot(
-            inv.astype(BF16),
-            concat([diagonal(mix.astype(BF16)), diagonal(piece(query_unit, u))], axis=1),
-        ).astype(BF16)
-        for inv, mix, u in zip(inverse, mixed, units)
+        part + dot(s, spread_pair(part.astype(BF16))) for s, part in zip(step, solved)
+    ]
+    solved = [
+        (part + dot(s, spread_pair(part.astype(BF16)))).astype(BF16)
+        for s, part in zip(square, solved)
     ]
     nothing = jnp.zeros((CHUNK, PAIR), BF16)
     lane = lax.broadcasted_iota(jnp.int32, (HEAD, 2 * PAIR), 1)
@@ -295,11 +314,24 @@
     own_map[...] = own_total
 
     pl.semaphore_wait(barrier, n_sp + n_tp - 2)
-    pair_copy = pltpu.make_async_remote_copy(
-        src_ref=own_map, dst_ref=partner_map, send_sem=pair_sem.at[0], recv_sem=pair_sem.at[1],
-        device_id=(sp + 1 - 2 * parity, tp), device_id_type=MESH,
-    )
-    pair_copy.start()
+    origin = group == 0
+    leads = origin & first_member
+
+    def pair_part(side):
+        span_of = pl.ds(side * HEAD, HEAD)
+        return pltpu.make_async_remote_copy(
+            src_ref=own_map.at[span_of], dst_ref=partner_map.at[span_of],
+            send_sem=pair_sem.at[side], recv_sem=pair_sem.at[2 + side],
+            device_id=(sp + 1 - 2 * parity, tp), device_id_type=MESH,
+        )
+
+    @pl.when((group > 0) | first_member)
+    def _():
+        pair_part(0).start()
+
+    @pl.when(group > 0)
+    def _():
+        pair_part(1).start()
 
     arrive("cv", "cg")
     both = concat([cv_buf[...], cg_buf[...]], axis=1)
@@ -321,12 +353,11 @@
 
     extended[halo_rows:, :] = conv_rows.astype(F32)
 
-    arrive("r", "g", "hgain")
-    receptance, gate = kept(dot(normed, r_buf[...])), kept(dot(normed, g_buf[...]))
+    arrive("r")
+    receptance = kept(project(r_buf))
     left_read = receptance * jnp.exp(cum - mid)
     query_read = left_read * from_start
     left_read = left_read.astype(BF16)
-    gate = jax.nn.sigmoid(gate) * hgain[...]
     zeros = jnp.zeros((PAIR, PAIR), BF16)
     products = [dot(piece(left_read, u), right, NT) for u, right in zip(units, rights)]
     reads = []
@@ -370,49 +401,72 @@
             out.append(dot(concat([move_part, move_part], axis=1), right))
         return concat(out, axis=1)
 
-    pair_copy.wait()
-    mine, theirs = own_total.astype(F32), partner_map[...].astype(F32)
-    early = jnp.where(first_member, mine, theirs).astype(WIRE)
-    late = jnp.where(first_member, theirs, mine).astype(WIRE)
-    joined = [
-        dot(move, spread_pair(concat([add, keep], axis=1)))
-        for move, add, keep in zip(by_pair(late[HEAD:]), by_pair(early[:HEAD]), by_pair(early[HEAD:]))
-    ]
-    pair_map[:HEAD] = (
-        concat([part[:, :PAIR] for part in joined], axis=1) + late[:HEAD].astype(F32)
-    ).astype(WIRE)
-    pair_map[HEAD:] = concat([part[:, PAIR:] for part in joined], axis=1).astype(WIRE)
+    early_map[...] = own_map[...]
+
+    @pl.when(parity == 1)
+    def _():
+        pair_part(0).wait_recv()
+        early_map[:HEAD] = partner_map[:HEAD]
+
+    def join(lead, follow, side):
+        moved = chain(lead[side * HEAD:(side + 1) * HEAD].astype(F32), follow[HEAD:])
+        if side == 0:
+            moved = moved + follow[:HEAD].astype(F32)
+        pair_map[side * HEAD:(side + 1) * HEAD] = moved.astype(WIRE)
+
+    @pl.when(origin & (parity == 1))
+    def _():
+        join(early_map, own_map, 0)
+
+    @pl.when(group > 0)
+    def _():
+        pair_part(1).wait_recv()
+
+    @pl.when((group > 0) & (parity == 1))
+    def _():
+        early_map[HEAD:] = partner_map[HEAD:]
+        join(early_map, own_map, 0)
+        join(early_map, own_map, 1)
+
+    @pl.when((group > 0) & first_member)
+    def _():
+        pair_part(0).wait_recv()
+        join(own_map, partner_map, 0)
+        join(own_map, partner_map, 1)
 
     hops = []
     while 2 ** len(hops) < groups:
         hops.append(2 ** len(hops))
 
-    def hop(source, k, side):
+    def hop(source, k, side, member=parity):
         span_of = pl.ds(side * HEAD, HEAD)
         return pltpu.make_async_remote_copy(
             src_ref=source.at[span_of], dst_ref=maps.at[k, span_of],
             send_sem=map_send.at[2 * k + side], recv_sem=map_recv.at[2 * k + side],
-            device_id=(sp + 2 * hops[k], tp), device_id_type=MESH,
+            device_id=(2 * (group + hops[k]) + member, tp), device_id_type=MESH,
+        )
+
+    def hop_across(k):
+        return pltpu.make_async_remote_copy(
+            src_ref=pair_map.at[pl.ds(0, HEAD)], dst_ref=maps.at[k, pl.ds(0, HEAD)],
+            send_sem=cross_send.at[k], recv_sem=map_recv.at[2 * k],
+            device_id=(2 * hops[k], tp), device_id_type=MESH,
         )
 
     sends = []
     for k, ahead in enumerate(hops):
         reached = group + ahead < groups
-        if k == 0:
-            sends.append((k, reached, pair_map, 0))
-            sends.append((k, reached & (group >= 1), pair_map, 1))
-        else:
-            sends.append((0, group == 0, pair_map, 0, k))
-            sends.append((k, reached & (group >= 1), windows.at[k], 0))
-            if 2 * ahead < groups:
-                sends.append((k, reached & (group >= ahead), windows.at[k], 1))
+        sends.append((0, origin & (parity == 1), hop_across(k)))
+        sends.append((0, origin & (parity == 1), hop(pair_map, k, 0)))
+        source = pair_map if k == 0 else windows.at[k]
+        sends.append((k, reached & (group >= 1), hop(source, k, 0)))
+        if 2 * ahead < groups:
+            sends.append((k, reached & (group >= ahead), hop(source, k, 1)))
 
     def send_step(step):
-        for when, allowed, source, side, *target in sends:
+        for when, allowed, copy in sends:
             if when == step:
-                @pl.when(allowed)
-                def _():
-                    hop(source, target[0] if target else step, side).start()
+                pl.when(allowed)(copy.start)
 
     if hops:
         send_step(0)
@@ -426,6 +480,21 @@
     def _():
         extended[:halo_rows, :] = jnp.zeros((halo_rows, channels), F32)
 
+
+    def fold(block):
+        for g in range(groups_of):
+            lanes = slice(g * PAIR, (g + 1) * PAIR)
+            right = spread_pair(concat([block[:HEAD, lanes], block[HEAD:, lanes]], axis=1))
+            moved = dot(carried[:, lanes], right)
+            local_read[:, lanes] = local_read[:, lanes] + moved[:, :PAIR]
+            carried[:, lanes] = moved[:, PAIR:].astype(BF16)
+
+    @pl.when(parity == 1)
+    def _():
+        fold(early_map)
+
+    arrive("g", "hgain")
+    gate = jax.nn.sigmoid(kept(project(g_buf))) * hgain[...]
     arrive("taps", "ggain", "gshift")
     tap_count = taps.shape[0]
     total = jnp.zeros((rows, channels), F32)
@@ -439,10 +508,20 @@
 
     span = rows // n_tp
 
+    def peer(step):
+        if n_tp & (n_tp - 1):
+            return lax.rem(tp + step, n_tp), lax.rem(tp - step + n_tp, n_tp)
+        other, bit = tp, 1
+        while bit < n_tp:
+            if step & bit:
+                other = other + bit - 2 * bit * lax.rem(tp // bit, 2)
+            bit *= 2
+        return other, other
+
     def spread(source, slots, send, recv):
         started = []
         for step in range(1, n_tp):
-            target = lax.rem(tp + step, n_tp)
+            target = peer(step)[0]
             begin = pl.multiple_of(target * span, span)
             copy = pltpu.make_async_remote_copy(
                 src_ref=source.at[pl.ds(begin, span)], dst_ref=slots.at[step],
@@ -457,36 +536,38 @@
 
     own = pl.multiple_of(tp * span, span)
 
-    def gather(result, source, slots, arriving, weight, depth):
-        result = result + dot(
-            source[pl.ds(own, span)], weight[pl.ds(pl.multiple_of(tp * depth, depth), depth)]
-        )
+    def gather(result, source, slots, arriving, weight, depth, offset, count):
+        def rows_of(owner):
+            return pl.ds(pl.multiple_of(owner * depth + offset, PAIR), count)
+
+        result = result + dot(source[pl.ds(own, span)], weight[rows_of(tp)])
         for step in range(1, n_tp):
             arriving[step - 1].wait_recv()
-            begin = lax.rem(tp - step + n_tp, n_tp) * depth
-            result = result + dot(
-                slots[step], weight[pl.ds(pl.multiple_of(begin, depth), depth)]
-            )
+            result = result + dot(slots[step], weight[rows_of(peer(step)[1])])
         return result
 
-    state[...] = jnp.zeros_like(state)
+    entered[...] = jnp.zeros_like(entered)
     for k, ahead in enumerate(hops):
+        final = group < 2 * ahead
+        following = 2 * ahead
+
         @pl.when(group >= ahead)
         def _():
             hop(pair_map, k, 0).wait_recv()
-            arrived = maps[k, :HEAD].astype(F32)
-            state[...] = arrived if k == 0 else chain(arrived, reach[...]) + state[...]
-
-        if 2 * ahead < groups:
-            @pl.when(group >= 2 * ahead)
+
+        @pl.when((group >= ahead) & final)
+        def _():
+            entered[...] = maps[k, :HEAD]
+
+        if following < groups:
+            @pl.when(group >= ahead)
             def _():
-                hop(pair_map, k, 1).wait_recv()
-                further = maps[k, HEAD:]
-                if k > 0:
-                    further = chain(further.astype(F32), reach[...]).astype(WIRE)
-                reach[...] = further
-
-            following = 2 * ahead
+                arrived = maps[k, :HEAD].astype(F32)
+                state[...] = arrived if k == 0 else chain(arrived, reach[...]) + state[...]
+
+            @pl.when((group == 0) & (k == 0))
+            def _():
+                state[...] = jnp.zeros_like(state)
 
             @pl.when((group >= 1) & (group + following < groups))
             def _():
@@ -495,46 +576,72 @@
                 ).astype(WIRE)
 
             if 2 * following < groups:
+                @pl.when(group >= following)
+                def _():
+                    hop(pair_map, k, 1).wait_recv()
+                    further = maps[k, HEAD:]
+                    if k > 0:
+                        further = chain(further.astype(F32), reach[...]).astype(WIRE)
+                    reach[...] = further
+
                 @pl.when((group >= following) & (group + following < groups))
                 def _():
                     windows[k + 1, HEAD:] = chain(
                         reach[...].astype(F32), pair_map[HEAD:]
                     ).astype(WIRE)
+            else:
+                @pl.when(group >= following)
+                def _():
+                    hop(pair_map, k, 1).wait_recv()
 
             send_step(k + 1)
 
-    behind = chain(state[...], early[HEAD:]) + early[:HEAD].astype(F32)
-    entering = jnp.where(first_member, state[...], behind).astype(BF16)
-    centred = local_read[...] + concat(
-        [
-            dot(carried[:, g * PAIR:(g + 1) * PAIR], diagonal(part))
-            for g, part in enumerate(by_pair(entering))
-        ],
-        axis=1,
-    )
-    head_means = jnp.where(same_head, 1.0 / HEAD, 0.0).astype(BF16)
-    scaled = centred * lax.rsqrt(dot((centred * centred).astype(BF16), head_means) + HEAD_EPS)
-    mix_out[...] = (scaled * gate).astype(BF16)
-    mix_copies = spread(mix_out, mix_slots, mix_send, mix_recv)
+            @pl.when(group >= following)
+            def _():
+                fold(maps.at[k])
+
+    head_means = jnp.where(head_blocks(PAIR), 1.0 / HEAD, 0.0).astype(BF16)
+    mix_copies = []
+    lanes_of = [slice(g * PAIR, (g + 1) * PAIR) for g in range(groups_of)]
+    centred = [
+        local_read[:, lanes] + dot(carried[:, lanes], diagonal(part))
+        for lanes, part in zip(lanes_of, by_pair(entered[...]))
+    ]
+    power = [dot((read * read).astype(BF16), head_means) for read in centred]
+    for g, lanes in enumerate(lanes_of):
+        scaled = centred[g] * lax.rsqrt(power[g] + HEAD_EPS)
+        mix_out[g] = (scaled * gate[:, lanes]).astype(BF16)
+        mix_copies.append(
+            spread(mix_out.at[g], mix_slots.at[g], mix_send.at[g], mix_recv.at[g])
+        )
     arrive("co")
     result = gather(
-        jnp.zeros(out.shape, F32), conv_out, conv_slots, conv_copies, co_buf, channels
+        jnp.zeros(out.shape, F32), conv_out, conv_slots, conv_copies, co_buf, channels, 0, channels
     )
 
     arrive("ao")
-    result = gather(result, mix_out, mix_slots, mix_copies, ao_buf, width)
+    for g in range(groups_of):
+        result = gather(
+            result, mix_out.at[g], mix_slots.at[g], mix_copies[g], ao_buf, width, g * PAIR, PAIR
+        )
     out[...] = result.astype(BF16)
-    for copy in conv_copies + mix_copies:
+    for copy in sum(mix_copies, conv_copies):
         copy.wait_send()
 
     @pl.when(has_next)
     def _():
         halo_copy.wait_send()
 
-    for when, allowed, source, side, *target in sends:
-        @pl.when(allowed)
-        def _():
-            hop(source, target[0] if target else when, side).wait_send()
+    for _, allowed, copy in sends:
+        pl.when(allowed)(copy.wait_send)
+
+    @pl.when((group > 0) | first_member)
+    def _():
+        pair_part(0).wait_send()
+
+    @pl.when(group > 0)
+    def _():
+        pair_part(1).wait_send()
 
 
 def local(
@@ -589,18 +696,22 @@
             pltpu.VMEM(map_shape, WIRE),
             pltpu.VMEM(map_shape, WIRE),
             pltpu.VMEM(map_shape, WIRE),
+            pltpu.VMEM(map_shape, WIRE),
             pltpu.VMEM((hop_count,) + map_shape, WIRE),
             pltpu.VMEM((hop_count,) + map_shape, WIRE),
             pltpu.VMEM((HEAD, width), F32),
             pltpu.VMEM((HEAD, width), WIRE),
+            pltpu.VMEM((HEAD, width), WIRE),
             pltpu.VMEM((rows, width), F32),
             pltpu.VMEM((rows, width), BF16),
             pltpu.VMEM((rows, channels), BF16),
-            pltpu.VMEM((rows, width), BF16),
+            pltpu.VMEM((width // PAIR, rows, PAIR), BF16),
             pltpu.VMEM((n_tp, span, channels), BF16),
-            pltpu.VMEM((n_tp, span, width), BF16),
-            dma((24,)), dma((2,)), dma((2,)), dma((2 * hop_count,)), dma((2 * hop_count,)),
-            dma((n_tp,)), dma((n_tp,)), dma((n_tp,)), dma((n_tp,)),
+            pltpu.VMEM((width // PAIR, n_tp, span, PAIR), BF16),
+            dma((24,)), dma((2,)), dma((4,)), dma((2 * hop_count,)), dma((2 * hop_count,)),
+            dma((hop_count,)),
+            dma((n_tp,)), dma((n_tp,)),
+            dma((width // PAIR, n_tp)), dma((width // PAIR, n_tp)),
         ],
         compiler_params=pltpu.CompilerParams(
             collective_id=0, has_side_effects=True, vmem_limit_bytes=VMEM_LIMIT

time: 20.9 us -> 19.8 us (0.947)
  Pallas kernels: 20 us -> 18.9 us
    pallas_call x1, Pallas kernels: 20 us -> 18.9 us  [local(): pl.pallas_call(functools.partial(layer_kernel, n_sp, n_tp), name='layer',...]
where the time goes in v3:
time: 19.8 us; the launch traced here: 19.6 us
  Pallas kernels  18.9 us (95%)
  local copies, waits for them, and re-layouts  0.71 us (4%)
    pallas_call x1, Pallas kernels, local(): pl.pallas_call(functools.partial(layer_kernel, n_sp, n_tp), name='layer',...  18.9 us
    unnamed x1, local copies, waits for them, and re-layouts  0.71 us

profile of v3, /device:TPU:25, one launch (start us, length us, event | category | flops | bytes accessed | tf_op | source)
XLA Modules:
  0.0 19.6 jit_solution(18434734110983049780)
XLA Ops:
  0.0 18.9 %layer.1 = bf16[64,2048]{1,0:T(8,128)(2,1)S(1)} custom-call(f32[1,2048]{1,0:T(1,128)} %bitcast.6, f32[1,256]{1,0:T(1,128)} %bitcast.7, f32[1,256]{1,0:T(1,128)} %bitcast.8, f32[31,128]{1,0:T(8,128)} %taps_hbm.1, f32[1,128]{1,0:T(1,128)} %bitcast.10, f32[1,128]{1,0:T(1,128)} %bitcast.11, f32[1,256]{1,0:T(1,128)} %bitcast.9, bf16[256,2048]{1,0:T(8,128)(2,1)} %tok_hbm.1, ...), custom_call_target="tpu_custom_call" | custom-call | tf_op jit(solution)/shard_map/layer/pallas_call | solution.py:679
  18.9 0.7 %copy.22 = bf16[64,2048]{1,0:T(8,128)(2,1)} copy(bf16[64,2048]{1,0:T(8,128)(2,1)S(1)} %layer.1) | data formatting | bytes 524288

commit v4 on v3

--- a/solution.py
+++ b/solution.py
@@ -114,9 +114,15 @@
         taps=(taps_hbm, taps), ggain=(ggain_hbm, ggain), gshift=(gshift_hbm, gshift),
         hgain=(hgain_hbm, hgain), co=(wco, co_buf), ao=(wao, ao_buf),
     )
+    together = (
+        ("gain", "tok0"), ("tok1",), ("k", "d"), ("bias", "shift", "extra", "kgain", "e"), ("v",),
+        ("cv", "cg"), ("r",), ("taps", "ggain", "gshift"), ("g", "hgain"), ("co",), ("ao",),
+    )
     copies = {}
-    for index, (key, (source, buffer)) in enumerate(order.items()):
-        copies[key] = pltpu.make_async_copy(source, buffer, weight_sem.at[index])
+    for index, keys in enumerate(together):
+        for key in keys:
+            source, buffer = order[key]
+            copies[key] = pltpu.make_async_copy(source, buffer, weight_sem.at[index])
 
     def begin(*keys):
         for key in keys:
@@ -147,9 +153,8 @@
     group, parity = sp // 2, lax.rem(sp, 2)
     first_member = parity == 0
     quarters = []
-    arrive("gain")
     for index, key in enumerate(token_keys):
-        arrive(key)
+        arrive(*(("gain", key) if index == 0 else (key,)))
         x = tok[index * part:(index + 1) * part].astype(F32)
         quarters.append(
             (
@@ -169,8 +174,7 @@
 
     arrive("k", "d")
     key_all, slope = kept(dot(normed, k_buf[...])), kept(dot(normed, d_buf[...]))
-    arrive("bias", "shift", "extra", "kgain", "e", "v")
-    begin("co", "ao")
+    arrive("bias", "shift", "extra", "kgain", "e")
     rate = kept(project(e_buf))
     same_head = head_blocks(width)
     ones = jnp.where(same_head, 1.0, 0.0).astype(BF16)
@@ -186,9 +190,7 @@
     )
     unit = key_all * kgain[...]
     unit = unit * lax.rsqrt(dot((unit * unit).astype(BF16), ones) + KEY_EPS)
-    value = project(v_buf).astype(BF16)
     erase = -(unit * jax.nn.sigmoid(rate))
-    value_high, value_low = split(dot(value, centre))
     chunks = rows // CHUNK
     groups_of = width // PAIR
 
@@ -229,12 +231,18 @@
     products = [dot(piece(left_unit, u), right, NT) for u, right in zip(units, rights)]
     lower = [jnp.where(strict, product[:, :PAIR], 0.0) for product in products]
     mixes = [jnp.where(strict, product[:, PAIR:], 0.0).astype(BF16) for product in products]
-    value_diagonals = [
-        concat([diagonal(piece(value_high, u)), diagonal(piece(value_low, u))]) for u in units
-    ]
-    mixed = [
-        dot(concat([mix, mix], axis=1), both) for mix, both in zip(mixes, value_diagonals)
-    ]
+    arrive("v")
+    begin("co", "ao")
+    slices = [slice(b, b + 2 * PAIR) for b in range(0, normed.shape[1], 2 * PAIR)]
+    value_sums = [None, None]
+
+    def value_some(count):
+        for span in [slices.pop(0) for _ in range(min(count, len(slices)))]:
+            for index, half in enumerate(halves):
+                part_of = dot(half[:, span], v_buf[span, :])
+                held = value_sums[index]
+                value_sums[index] = part_of if held is None else held + part_of
+
     def within(size):
         return (row // size) == (col // size)
 
@@ -245,26 +253,36 @@
     inverse = [eye + s for s in step]
     narrow = [s.astype(BF16) for s in step]
     square = [dot(s, diagonal(s)).astype(BF16) for s in narrow]
+    value_some(3)
     inverse = [
         inv + dot(s, diagonal(inv.astype(BF16))) for inv, s in zip(inverse, square)
     ]
+    value_some(3)
     narrow = [inv.astype(BF16) for inv in inverse]
     step = [
         dot(inv, diagonal(jnp.where(within(16) & ~within(4), low, 0.0).astype(BF16))).astype(BF16)
         for inv, low in zip(narrow, lower)
     ]
+    value_some(len(slices))
     both = [powers(s, inv) for s, inv in zip(step, narrow)]
+    value_high, value_low = split(dot(concat(value_sums).astype(BF16), centre))
     inverse = [inv + pair[:, :PAIR] for inv, pair in zip(inverse, both)]
     square = [pair[:, PAIR:].astype(BF16) for pair in both]
     inverse = [
         (inv + dot(s, diagonal(inv.astype(BF16)))).astype(BF16) for inv, s in zip(inverse, square)
     ]
+    value_diagonals = [
+        concat([diagonal(piece(value_high, u)), diagonal(piece(value_low, u))]) for u in units
+    ]
+    mixed = [
+        dot(concat([mix, mix], axis=1), held) for mix, held in zip(mixes, value_diagonals)
+    ]
+    outer = [diagonal(jnp.where(within(16), 0.0, low).astype(BF16)) for low in lower]
+    step = [dot(inv, far).astype(BF16) for inv, far in zip(inverse, outer)]
     sides = [
         spread_pair(concat([mix.astype(BF16), piece(query_unit, u)], axis=1))
         for mix, u in zip(mixed, units)
     ]
-    outer = [diagonal(jnp.where(within(16), 0.0, low).astype(BF16)) for low in lower]
-    step = [dot(inv, far).astype(BF16) for inv, far in zip(inverse, outer)]
     solved = [dot(inv, side) for inv, side in zip(inverse, sides)]
     square = [dot(s, diagonal(s)).astype(BF16) for s in step]
     solved = [
@@ -519,31 +537,36 @@
         return other, other
 
     def spread(source, slots, send, recv):
-        started = []
-        for step in range(1, n_tp):
+        started = {}
+        for step in list(range(2, n_tp, 2)) + list(range(n_tp - 1 + n_tp % 2, 0, -2)):
+            if step >= n_tp:
+                continue
             target = peer(step)[0]
             begin = pl.multiple_of(target * span, span)
-            copy = pltpu.make_async_remote_copy(
-                src_ref=source.at[pl.ds(begin, span)], dst_ref=slots.at[step],
-                send_sem=send.at[step], recv_sem=recv.at[step],
+            started[step] = pltpu.make_async_remote_copy(
+                src_ref=source.at[pl.ds(begin, span)], dst_ref=slots.at[step - 1],
+                send_sem=send.at[step - 1], recv_sem=recv.at[step - 1],
                 device_id=(sp, target), device_id_type=MESH,
             )
-            copy.start()
-            started.append(copy)
+            started[step].start()
         return started
 
     conv_copies = spread(conv_out, conv_slots, conv_send, conv_recv)
 
     own = pl.multiple_of(tp * span, span)
 
-    def gather(result, source, slots, arriving, weight, depth, offset, count):
-        def rows_of(owner):
-            return pl.ds(pl.multiple_of(owner * depth + offset, PAIR), count)
-
-        result = result + dot(source[pl.ds(own, span)], weight[rows_of(tp)])
+    def gather(result, source, slots, arriving, weight, depth, lanes):
+        def take(result, rows, owner):
+            for begin in range(0, depth, lanes):
+                left = rows[:, begin:begin + lanes]
+                offset = pl.multiple_of(owner * depth + begin, lanes)
+                result = result + dot(left, weight[pl.ds(offset, lanes)])
+            return result
+
+        result = take(result, source[pl.ds(own, span)], tp)
         for step in range(1, n_tp):
-            arriving[step - 1].wait_recv()
-            result = result + dot(slots[step], weight[rows_of(peer(step)[1])])
+            arriving[step].wait_recv()
+            result = take(result, slots[step - 1], peer(step)[1])
         return result
 
     entered[...] = jnp.zeros_like(entered)
@@ -601,7 +624,6 @@
                 fold(maps.at[k])
 
     head_means = jnp.where(head_blocks(PAIR), 1.0 / HEAD, 0.0).astype(BF16)
-    mix_copies = []
     lanes_of = [slice(g * PAIR, (g + 1) * PAIR) for g in range(groups_of)]
     centred = [
         local_read[:, lanes] + dot(carried[:, lanes], diagonal(part))
@@ -610,23 +632,19 @@
     power = [dot((read * read).astype(BF16), head_means) for read in centred]
     for g, lanes in enumerate(lanes_of):
         scaled = centred[g] * lax.rsqrt(power[g] + HEAD_EPS)
-        mix_out[g] = (scaled * gate[:, lanes]).astype(BF16)
-        mix_copies.append(
-            spread(mix_out.at[g], mix_slots.at[g], mix_send.at[g], mix_recv.at[g])
-        )
+        mix_out[:, lanes] = (scaled * gate[:, lanes]).astype(BF16)
+    mix_copies = spread(mix_out, mix_slots, mix_send, mix_recv)
     arrive("co")
     result = gather(
-        jnp.zeros(out.shape, F32), conv_out, conv_slots, conv_copies, co_buf, channels, 0, channels
+        jnp.zeros(out.shape, F32), conv_out, conv_slots, conv_copies, co_buf, channels, channels
     )
 
     arrive("ao")
-    for g in range(groups_of):
-        result = gather(
-            result, mix_out.at[g], mix_slots.at[g], mix_copies[g], ao_buf, width, g * PAIR, PAIR
-        )
+    result = gather(result, mix_out, mix_slots, mix_copies, ao_buf, width, PAIR)
     out[...] = result.astype(BF16)
-    for copy in sum(mix_copies, conv_copies):
-        copy.wait_send()
+    for step in range(1, n_tp):
+        conv_copies[step].wait_send()
+        mix_copies[step].wait_send()
 
     @pl.when(has_next)
     def _():
@@ -705,13 +723,12 @@
             pltpu.VMEM((rows, width), F32),
             pltpu.VMEM((rows, width), BF16),
             pltpu.VMEM((rows, channels), BF16),
-            pltpu.VMEM((width // PAIR, rows, PAIR), BF16),
-            pltpu.VMEM((n_tp, span, channels), BF16),
-            pltpu.VMEM((width // PAIR, n_tp, span, PAIR), BF16),
-            dma((24,)), dma((2,)), dma((4,)), dma((2 * hop_count,)), dma((2 * hop_count,)),
+            pltpu.VMEM((rows, width), BF16),
+            pltpu.VMEM((n_tp - 1, span, channels), BF16),
+            pltpu.VMEM((n_tp - 1, span, width), BF16),
+            dma((11,)), dma((2,)), dma((4,)), dma((2 * hop_count - 1,)), dma((2 * hop_count - 1,)),
             dma((hop_count,)),
-            dma((n_tp,)), dma((n_tp,)),
-            dma((width // PAIR, n_tp)), dma((width // PAIR, n_tp)),
+            dma((n_tp - 1,)), dma((n_tp - 1,)), dma((n_tp - 1,)), dma((n_tp - 1,)),
         ],
         compiler_params=pltpu.CompilerParams(
             collective_id=0, has_side_effects=True, vmem_limit_bytes=VMEM_LIMIT

time: 19.8 us -> 19.4 us (0.980)
  Pallas kernels: 18.9 us -> 18.5 us
    pallas_call x1, Pallas kernels: 18.9 us -> 18.5 us  [local(): pl.pallas_call(functools.partial(layer_kernel, n_sp, n_tp), name='layer',...]
where the time goes in v4:
time: 19.4 us; the launch traced here: 19.2 us
  Pallas kernels  18.5 us (95%)
  local copies, waits for them, and re-layouts  0.71 us (4%)
    pallas_call x1, Pallas kernels, local(): pl.pallas_call(functools.partial(layer_kernel, n_sp, n_tp), name='layer',...  18.5 us
    unnamed x1, local copies, waits for them, and re-layouts  0.71 us

profile of v4, /device:TPU:25, one launch (start us, length us, event | category | flops | bytes accessed | tf_op | source)
XLA Modules:
  0.0 19.2 jit_solution(12605669771735779094)
XLA Ops:
  0.0 18.5 %layer.1 = bf16[64,2048]{1,0:T(8,128)(2,1)S(1)} custom-call(f32[1,2048]{1,0:T(1,128)} %bitcast.6, f32[1,256]{1,0:T(1,128)} %bitcast.7, f32[1,256]{1,0:T(1,128)} %bitcast.8, f32[31,128]{1,0:T(8,128)} %taps_hbm.1, f32[1,128]{1,0:T(1,128)} %bitcast.10, f32[1,128]{1,0:T(1,128)} %bitcast.11, f32[1,256]{1,0:T(1,128)} %bitcast.9, bf16[256,2048]{1,0:T(8,128)(2,1)} %tok_hbm.1, ...), custom_call_target="tpu_custom_call" | custom-call | tf_op jit(solution)/shard_map/layer/pallas_call | solution.py:697
  18.5 0.7 %copy.22 = bf16[64,2048]{1,0:T(8,128)(2,1)} copy(bf16[64,2048]{1,0:T(8,128)(2,1)S(1)} %layer.1) | data formatting | bytes 524288

commit v5 on v4

--- a/solution.py
+++ b/solution.py
@@ -99,7 +99,7 @@
     tok, shift, extra, cv_buf, cg_buf, k_buf, r_buf, d_buf, e_buf, v_buf, g_buf, co_buf, ao_buf,
     conv_in, extended, halo, own_map, partner_map, pair_map, early_map, maps, windows, state, reach, entered,
     local_read, carried, conv_out, mix_out, conv_slots, mix_slots,
-    weight_sem, halo_sem, pair_sem, map_send, map_recv, cross_send, conv_send, conv_recv, mix_send, mix_recv,
+    weight_sem, halo_sem, pair_sem, map_send, map_recv, conv_send, conv_recv, mix_send, mix_recv,
 ):
     sp, tp = lax.axis_index("sp"), lax.axis_index("tp")
     part = tok_hbm.shape[0] // TOKEN_PARTS
@@ -339,7 +339,7 @@
         span_of = pl.ds(side * HEAD, HEAD)
         return pltpu.make_async_remote_copy(
             src_ref=own_map.at[span_of], dst_ref=partner_map.at[span_of],
-            send_sem=pair_sem.at[side], recv_sem=pair_sem.at[2 + side],
+            send_sem=pair_sem.at[2], recv_sem=pair_sem.at[side],
             device_id=(sp + 1 - 2 * parity, tp), device_id_type=MESH,
         )
 
@@ -460,14 +460,14 @@
         span_of = pl.ds(side * HEAD, HEAD)
         return pltpu.make_async_remote_copy(
             src_ref=source.at[span_of], dst_ref=maps.at[k, span_of],
-            send_sem=map_send.at[2 * k + side], recv_sem=map_recv.at[2 * k + side],
+            send_sem=map_send.at[0], recv_sem=map_recv.at[2 * k + side],
             device_id=(2 * (group + hops[k]) + member, tp), device_id_type=MESH,
         )
 
     def hop_across(k):
         return pltpu.make_async_remote_copy(
             src_ref=pair_map.at[pl.ds(0, HEAD)], dst_ref=maps.at[k, pl.ds(0, HEAD)],
-            send_sem=cross_send.at[k], recv_sem=map_recv.at[2 * k],
+            send_sem=map_send.at[0], recv_sem=map_recv.at[2 * k],
             device_id=(2 * hops[k], tp), device_id_type=MESH,
         )
 
@@ -545,7 +545,7 @@
             begin = pl.multiple_of(target * span, span)
             started[step] = pltpu.make_async_remote_copy(
                 src_ref=source.at[pl.ds(begin, span)], dst_ref=slots.at[step - 1],
-                send_sem=send.at[step - 1], recv_sem=recv.at[step - 1],
+                send_sem=send.at[0], recv_sem=recv.at[step - 1],
                 device_id=(sp, target), device_id_type=MESH,
             )
             started[step].start()
@@ -726,9 +726,8 @@
             pltpu.VMEM((rows, width), BF16),
             pltpu.VMEM((n_tp - 1, span, channels), BF16),
             pltpu.VMEM((n_tp - 1, span, width), BF16),
-            dma((11,)), dma((2,)), dma((4,)), dma((2 * hop_count - 1,)), dma((2 * hop_count - 1,)),
-            dma((hop_count,)),
-            dma((n_tp - 1,)), dma((n_tp - 1,)), dma((n_tp - 1,)), dma((n_tp - 1,)),
+            dma((11,)), dma((2,)), dma((3,)), dma((1,)), dma((2 * hop_count - 1,)),
+            dma((1,)), dma((n_tp - 1,)), dma((1,)), dma((n_tp - 1,)),
         ],
         compiler_params=pltpu.CompilerParams(
             collective_id=0, has_side_effects=True, vmem_limit_bytes=VMEM_LIMIT

time: 19.4 us -> 19.3 us (level)
  no operation moved by 1% of the time
where the time goes in v5:
time: 19.3 us; the launch traced here: 19.1 us
  Pallas kernels  18.4 us (95%)
  local copies, waits for them, and re-layouts  0.71 us (4%)
    pallas_call x1, Pallas kernels, local(): pl.pallas_call(functools.partial(layer_kernel, n_sp, n_tp), name='layer',...  18.4 us
    unnamed x1, local copies, waits for them, and re-layouts  0.71 us

profile of v5, /device:TPU:25, one launch (start us, length us, event | category | flops | bytes accessed | tf_op | source)
XLA Modules:
  0.0 19.1 jit_solution(16941496222221264006)
XLA Ops:
  0.0 18.4 %layer.1 = bf16[64,2048]{1,0:T(8,128)(2,1)S(1)} custom-call(f32[1,2048]{1,0:T(1,128)} %bitcast.6, f32[1,256]{1,0:T(1,128)} %bitcast.7, f32[1,256]{1,0:T(1,128)} %bitcast.8, f32[31,128]{1,0:T(8,128)} %taps_hbm.1, f32[1,128]{1,0:T(1,128)} %bitcast.10, f32[1,128]{1,0:T(1,128)} %bitcast.11, f32[1,256]{1,0:T(1,128)} %bitcast.9, bf16[256,2048]{1,0:T(8,128)(2,1)} %tok_hbm.1, ...), custom_call_target="tpu_custom_call" | custom-call | tf_op jit(solution)/shard_map/layer/pallas_call | solution.py:697
  18.4 0.7 %copy.22 = bf16[64,2048]{1,0:T(8,128)(2,1)} copy(bf16[64,2048]{1,0:T(8,128)(2,1)S(1)} %layer.1) | data formatting | bytes 524288
